TPU v7x, 512 devices: a whole 4x8x8 slice. The times are simulated.
512 devices in a mesh: sp: 64 (over z, y), fs: 4 (over x), tp: 2 (over core).
Axes of the slice: x: 4, y: 8, z: 8, core: 2. Of those that a mesh axis runs over, the one named last changes fastest.
Arguments:
- recurrent_query: bfloat16 [4, 16384, 1024], P('fs', 'sp', 'tp'), may hold values from -6 to 6
- forget_logits: bfloat16 [4, 16384, 1024], P('fs', 'sp', 'tp'), may hold values from -6 to 6
- recurrent_value: bfloat16 [4, 16384, 1024], P('fs', 'sp', 'tp'), may hold values from -6 to 6
- forget_floor: float32 [2, 1024], P(None, 'tp'), may hold values from 0.8 to 1
- extra_log_decay: float32 [4, 16384, 8], P('fs', 'sp', 'tp'), may hold values from -1 to 0
- recurrent_norm_gain: float32 [1024], P('tp'), may hold values from 0.1 to 1.9
- attention_query: bfloat16 [4, 16384, 768], P('fs', 'sp', 'tp'), may hold values from -300 to 300
- latent: bfloat16 [4, 16384, 256], P('fs', 'sp'), may hold values from -6 to 6
- rotary_key: bfloat16 [4, 16384, 32], P('fs', 'sp'), may hold values from -15 to 15
- latent_norm_gain: float32 [256], replicated, may hold values from 0.1 to 1.9
- latent_up_weight: bfloat16 [256, 1024], replicated, may hold values from -0.375 to 0.375
- recurrent_output_weight: bfloat16 [1024, 2048], P('tp', 'fs'), may hold values from -0.1875 to 0.1875
- attention_output_weight: bfloat16 [512, 2048], P('tp', 'fs'), may hold values from -2 to 2
Outputs:
- mixed: bfloat16 [4, 16384, 2048], P('fs', ('sp', 'tp'))
- log_weight: float32 [4, 16384, 8], P('fs', 'sp', 'tp')
All inputs are finite; a program needn't handle non-finite values.
Results may differ from a plain program's by a relative error of at most 0.013.
The roundings to bfloat16 on the way count: a program that leaves them out, or rounds other values in their place, can miss the bound.
Values may be sent and summed in bfloat16 or wider, within the bound.
No kernel may reach another device: no remote copies, remote signals or barrier semaphores. Data moves between devices by JAX's collectives and lax.ppermute only.
A program may use at most 128 MiB of HBM per device.

v0:
```python
import math

import jax
import jax.numpy as jnp
from jax import lax
from jax.sharding import Mesh
from jax.sharding import PartitionSpec as P

HG_DK = 128
HG_DV = 128
NOPE = 64
ROPE = 32
VDIM = 64
HG_BLOCK = 64
TOK_DEV = 256
SP = ("sp_0", "sp_1")
SP_TP = ("sp_0", "sp_1", "tp")


norm_eps = 1e-06
rope_base = 10000.0
widest_span = 8
floor_score = -1e30


def neutral_like(shard, identity):
    return jax.tree.map(
        lambda part, zero: jnp.zeros_like(part) + jnp.asarray(zero, part.dtype), shard, identity
    )


def carried_in(shard, axes, combine, identity, reverse):
    before = start = neutral_like(shard, identity)
    so_far = shard
    for axis in reversed(axes):
        size, position = (lax.axis_size(axis), lax.axis_index(axis))
        pieces = jax.tree.map(
            lambda part, kind: lax.all_gather(part.astype(kind), axis),
            so_far,
            jax.tree.map(lambda a: jnp.bfloat16 if a.dtype == jnp.float32 else a.dtype, shard),
        )
        inside, so_far = (start, start)
        for k in reversed(range(size)) if reverse else range(size):
            passed = k > position if reverse else k < position
            so_far = combine(
                so_far, jax.tree.map(lambda part, own: part[k].astype(own.dtype), pieces, shard)
            )
            inside = jax.tree.map(lambda new, old: jnp.where(passed, new, old), so_far, inside)
        before = combine(inside, before)
    return before


def from_partner(value, axis, distance):
    mask = 2**distance
    pairs = [(source, source ^ mask) for source in range(lax.axis_size(axis))]
    return lax.ppermute(value, axis, pairs)


def sent_together(arrays, axis, dim, along):
    both = jnp.concatenate(arrays, axis=along)
    result, at, finished = (lax.all_gather(both, axis, axis=dim, tiled=True), 0, [])
    for a in arrays:
        finished.append(lax.slice_in_dim(result, at, at + a.shape[along], axis=along))
        at += a.shape[along]
    return tuple(finished)


def cut_along(shard, dim, size):
    before, after = (shard.shape[:dim], shard.shape[dim + 1 :])
    return jnp.moveaxis(shard.reshape(*before, size, -1, *after), dim, 0)


def sent_and_summed(shard, axis, dim):
    pieces = cut_along(shard, dim, lax.axis_size(axis))
    arrived = lax.all_to_all(pieces, axis, split_axis=0, concat_axis=0, tiled=True)
    return arrived.astype(jnp.float32).sum(axis=0)


def rope_tables(token_count, offset):
    places = offset + jnp.arange(token_count).astype(jnp.float32)
    pair_count = ROPE // 2
    inverse = rope_base ** (-jnp.arange(pair_count).astype(jnp.float32) / pair_count)
    angles = places[:, None] * inverse[None, :]
    return (jnp.cos(angles), jnp.sin(angles))


def rotate(tensor, cos_table, sin_table):
    half_width = tensor.shape[-1] // 2
    first_half = tensor[..., :half_width]
    second_half = tensor[..., half_width:]
    return jnp.concatenate(
        [
            first_half * cos_table - second_half * sin_table,
            first_half * sin_table + second_half * cos_table,
        ],
        axis=-1,
    )


def block_pass(queries, key_matrix, values, decay_logarithm, carried):
    length = queries.shape[0]
    blocks = length // HG_BLOCK

    def split_blocks(tensor):
        return tensor.reshape((blocks, HG_BLOCK) + tensor.shape[1:])

    lower_mask = jnp.tril(jnp.ones((HG_BLOCK, HG_BLOCK), dtype=bool))

    def advance(running_state, input_tuple):
        query_blk, key_tile, value_tile, decay_blk = input_tuple
        inner_block_term = jnp.cumsum(decay_blk, axis=0)
        damped_query = query_blk * jnp.exp(inner_block_term)
        key_decayed = key_tile * jnp.exp(-inner_block_term)
        cross_block_term = jnp.einsum("mcx,cxn->mcn", damped_query, running_state)
        scores = jnp.einsum("thk,shk->hts", damped_query, key_decayed)
        scores = jnp.where(lower_mask[None], scores, 0.0)
        intra_term = jnp.einsum("hts,shv->thv", scores, value_tile)
        decay_total = inner_block_term[-1]
        updated_state = jnp.exp(decay_total)[:, :, None] * running_state + jnp.einsum(
            "jrg,jrb->rgb", key_tile * jnp.exp(decay_total[None] - inner_block_term), value_tile
        )
        return (updated_state, cross_block_term + intra_term)

    final_state, outputs = lax.scan(
        advance,
        carried,
        (
            split_blocks(queries),
            split_blocks(key_matrix),
            split_blocks(values),
            split_blocks(decay_logarithm),
        ),
    )
    return (outputs.reshape((length,) + outputs.shape[2:]), final_state)


def gate_factors(forget_gate, spike_amount, gate_floor):
    decay_logarithm = (
        jnp.logaddexp(jnp.log(gate_floor), jnp.log1p(-gate_floor) + jax.nn.log_sigmoid(forget_gate))
        + spike_amount[:, :, None]
    )
    key_matrix = (1.0 - gate_floor) * jax.nn.sigmoid(-forget_gate)
    return (key_matrix, decay_logarithm)


def head_norm(outputs, gain):
    return (
        outputs * lax.rsqrt(jnp.mean(outputs * outputs, axis=-1, keepdims=True) + norm_eps) * gain
    )


def chain_combine(earlier, later):
    return (earlier[0] * later[0], later[0][:, :, None] * earlier[1] + later[1])


def local(
    recurrent_query,
    forget_logits,
    recurrent_value,
    forget_floor,
    extra_log_decay,
    recurrent_norm_gain,
    attention_query,
    latent,
    rotary_key,
    latent_norm_gain,
    latent_up_weight,
    recurrent_output_weight,
    attention_output_weight,
):
    span = min(lax.axis_size(SP), widest_span)
    seq_len = TOK_DEV * span
    sp_index = lax.axis_index(SP)
    local_place = sp_index % span
    seq_offset = sp_index * TOK_DEV % seq_len
    queries = recurrent_query[0].astype(jnp.float32)
    heads_here = queries.shape[1] // HG_DK
    queries = queries.reshape(TOK_DEV, heads_here, HG_DK)
    forget_gate = forget_logits[0].astype(jnp.float32).reshape(TOK_DEV, heads_here, HG_DK)
    values = recurrent_value[0].astype(jnp.float32).reshape(TOK_DEV, heads_here, HG_DV)
    summed = jnp.zeros((TOK_DEV, heads_here, HG_DV), jnp.float32)
    for direction in range(2):
        gate_floor = forget_floor[direction].reshape(heads_here, HG_DK)
        key_matrix, decay_logarithm = gate_factors(forget_gate, extra_log_decay[0], gate_floor)
        sorted_rows = [queries, key_matrix, values, decay_logarithm]
        if direction == 1:
            sorted_rows = [jnp.flip(member, axis=0) for member in sorted_rows]
        local_out, local_state = block_pass(
            sorted_rows[0],
            sorted_rows[1],
            sorted_rows[2],
            sorted_rows[3],
            jnp.zeros((heads_here, HG_DK, HG_DV), jnp.float32),
        )
        running_state = jnp.cumsum(sorted_rows[3], axis=0)
        boundary = local_place == (span - 1 if direction == 0 else 0)
        element = (
            jnp.where(boundary, 0.0, jnp.exp(running_state[-1])),
            jnp.where(boundary, 0.0, local_state),
        )
        identity = (
            jnp.ones((heads_here, HG_DK), jnp.float32),
            jnp.zeros((heads_here, HG_DK, HG_DV), jnp.float32),
        )
        if direction == 0:
            arriving_state = carried_in(element, SP, chain_combine, identity, False)
        else:
            arriving_state = carried_in(element, SP, chain_combine, identity, True)
        result = local_out + jnp.einsum(
            "mcx,cxn->mcn", sorted_rows[0] * jnp.exp(running_state), arriving_state[1]
        )
        if direction == 1:
            result = jnp.flip(result, axis=0)
        summed = summed + result
    normed = head_norm(summed, recurrent_norm_gain.reshape(heads_here, HG_DV))
    recurrent_out = normed.astype(jnp.bfloat16).reshape(TOK_DEV, heads_here * HG_DV)
    heads_att = attention_query.shape[2] // (NOPE + ROPE)
    head_query = attention_query[0].reshape(TOK_DEV, heads_att, NOPE + ROPE)
    cos_table, sin_table = rope_tables(TOK_DEV, seq_offset.astype(jnp.float32))
    query_rope = rotate(
        head_query[..., NOPE:].astype(jnp.float32), cos_table[:, None], sin_table[:, None]
    )
    query_all = jnp.concatenate([head_query[..., :NOPE], query_rope.astype(jnp.bfloat16)], axis=-1)
    latent_wide = latent[0].astype(jnp.float32)
    normed = (
        latent_wide
        * lax.rsqrt(jnp.mean(latent_wide * latent_wide, axis=-1, keepdims=True) + norm_eps)
        * latent_norm_gain
    ).astype(jnp.bfloat16)
    rotated_key = rotate(rotary_key[0].astype(jnp.float32), cos_table, sin_table).astype(
        jnp.bfloat16
    )
    width_here = heads_att * (NOPE + VDIM)
    w_here = lax.dynamic_slice_in_dim(
        latent_up_weight, lax.axis_index("tp") * width_here, width_here, 1
    )
    score_scale = (NOPE + ROPE) ** (-0.5)

    def attend_keys(carried, expanded, rotated):
        key_count = expanded.shape[0]
        expanded = expanded.reshape(key_count, heads_att, NOPE + VDIM)
        keys_all = jnp.concatenate(
            [
                expanded[..., :NOPE],
                jnp.broadcast_to(rotated[:, None, :], (key_count, heads_att, ROPE)),
            ],
            axis=-1,
        )
        values = expanded[..., NOPE:]
        scores = jnp.einsum("qhd,khd->hqk", query_all, keys_all, preferred_element_type=jnp.float32)
        scores = scores * score_scale
        row_peak, totals, weighted = carried
        new_peak = jnp.maximum(row_peak, jnp.max(scores, axis=-1))
        weights = jnp.exp(scores - new_peak[..., None])
        rescale = jnp.exp(row_peak - new_peak)
        totals = totals * rescale + jnp.sum(weights, axis=-1)
        weighted = weighted * rescale.T[:, :, None] + jnp.einsum(
            "hqk,khv->qhv", weights.astype(jnp.bfloat16), values, preferred_element_type=jnp.float32
        )
        return (new_peak, totals, weighted)

    initial = (
        jnp.full((heads_att, TOK_DEV), floor_score, jnp.float32),
        jnp.zeros((heads_att, TOK_DEV), jnp.float32),
        jnp.zeros((TOK_DEV, heads_att, VDIM), jnp.float32),
    )
    pieces = (normed, rotated_key)
    for bit_number in range(span.bit_length() - 1):
        partner = from_partner((pieces[0], pieces[1]), SP, bit_number)
        pieces = (
            jnp.concatenate([pieces[0], partner[0]], axis=0),
            jnp.concatenate([pieces[1], partner[1]], axis=0),
        )
    first_rows = pieces[0]
    rotated = pieces[1]
    key_count = first_rows.shape[0]
    key_block = math.gcd(key_count, max(TOK_DEV, 1024))
    grouped = (
        first_rows.reshape(key_count // key_block, key_block, first_rows.shape[1]),
        rotated.reshape(key_count // key_block, key_block, rotated.shape[1]),
    )

    def visit_block(running_state, block_parts):
        expanded = jnp.dot(block_parts[0], w_here, preferred_element_type=jnp.float32).astype(
            jnp.bfloat16
        )
        return (attend_keys(running_state, expanded, block_parts[1]), None)

    folded, unused = lax.scan(visit_block, initial, grouped)
    row_peak, totals, weighted = folded
    attention_attention_out = (
        (weighted / totals.T[:, :, None]).astype(jnp.bfloat16).reshape(TOK_DEV, heads_att * VDIM)
    )
    log_weight = (row_peak + jnp.log(totals)).T
    attention_out, log_weight = (attention_attention_out, log_weight)
    w_hg_full, w_att_full = sent_together(
        (recurrent_output_weight, attention_output_weight), "fs", 1, 0
    )
    rows_here = TOK_DEV // lax.axis_size("tp")
    mixed = sent_and_summed(
        (
            jnp.dot(recurrent_out, w_hg_full, preferred_element_type=jnp.float32)
            + jnp.dot(attention_out, w_att_full, preferred_element_type=jnp.float32)
        ).astype(jnp.bfloat16),
        "tp",
        0,
    ).astype(jnp.bfloat16)
    return (mixed.reshape(1, rows_here, mixed.shape[-1]), log_weight[None])


def solution(mesh):
    torus = Mesh(
        mesh.devices.reshape(8, 8, mesh.shape["fs"], mesh.shape["tp"]), ("sp_0", "sp_1", "fs", "tp")
    )
    in_specs = (
        P("fs", SP, "tp"),
        P("fs", SP, "tp"),
        P("fs", SP, "tp"),
        P(None, "tp"),
        P("fs", SP, "tp"),
        P("tp"),
        P("fs", SP, "tp"),
        P("fs", SP, None),
        P("fs", SP, None),
        P(),
        P(),
        P("tp", "fs"),
        P("tp", "fs"),
    )
    out_specs = (P("fs", SP_TP, None), P("fs", SP, "tp"))
    return jax.shard_map(local, mesh=torus, in_specs=in_specs, out_specs=out_specs, check_vma=False)
```

profile of v0, /device:TPU:1, one launch (start us, length us, event | category | flops | bytes accessed | tf_op | source)
XLA Modules:
  0.0 277.5 jit_solution(1234217350554984415)
XLA Ops:
  8.1 1.1 copy.193
  9.3 1.1 copy.199
  10.6 1.8 add_bitcast_fusion
  13.1 1.0 copy.212
  14.2 3.0 %rev.17 = f32[256,4,128]{0,2,1:T(8,128)} reverse(f32[256,4,128]{0,2,1:T(8,128)S(1)} %broadcast_multiply_fusion), dimensions={0} | reverse | bytes 1048576 | tf_op jit(solution)/shard_map/jit(_flip)/rev | solution.py:187
  17.2 2.1 copy.213
  20.1 1.2 copy.209
  21.4 2.7 rev.19
  24.1 2.9 %rev.18 = bf16[256,4,128]{0,2,1:T(8,128)(2,1)} reverse(bf16[256,4,128]{0,2,1:T(8,128)(2,1)S(1)} %bitcast.684), dimensions={0} | reverse | bytes 524288 | tf_op jit(solution)/shard_map/jit(_flip)/rev | solution.py:187
  27.0 1.1 copy.214
  28.1 0.8 broadcast.241.clone3
  28.9 14.4 %while.42 = (s32[]{:T(128)}, f32[4,128,128]{2,1,0:T(8,128)S(1)}, f32[4,64,4,128]{3,1,0,2:T(8,128)}, f32[4,64,4,128]{3,1,0,2:T(8,128)}, f32[4,64,4,128]{3,2,1,0:T...) while((s32[]{:T(128)}, f32[4,128,128]{2,1,0:T(8,128)S(1)}, ...), condition=%wide.region_7.8_spmd.clone, body=%wide.region_5.7_spmd.clone.sunk | while | flops 27807748 | bytes 2974328 | solution.py:124
  28.9 1.0 constant_dynamic-slice_fusion.4
  30.0 1.1 bitcast_multiply_fusion.8
  32.5 1.0 constant_dynamic-slice_fusion.4
  33.6 1.1 bitcast_multiply_fusion.8
  35.0 0.8 fusion.386
  36.2 1.0 constant_dynamic-slice_fusion.4
  37.3 1.1 bitcast_multiply_fusion.8
  39.8 1.0 constant_dynamic-slice_fusion.4
  40.9 1.1 bitcast_multiply_fusion.8
  44.1 1.0 copy.196
  45.1 1.0 copy.194
  46.2 1.0 copy.200
  47.7 2.0 neg.73
  49.7 2.0 reshape.625
  52.0 2.4 select_add_fusion.1
  54.4 0.9 broadcast.241.clone3.1
  55.3 10.1 %while.41 = (s32[]{:T(128)}, f32[4,128,128]{2,1,0:T(8,128)S(1)}, f32[4,64,4,128]{3,1,0,2:T(8,128)}, f32[4,64,4,128]{3,2,1,0:T(4,128)S(1)}, f32[4,64,4,128]{3,2,1...) while((s32[]{:T(128)}, f32[4,128,128]{2,1,0:T(8,128)S(1)}, ...), condition=%wide.region_2.3_spmd.clone, body=%wide.region_0.2_spmd.clone.sunk | while | flops 27807748 | bytes 2450040 | solution.py:124
  55.3 1.0 bitcast_multiply_fusion.7
  57.9 1.0 bitcast_multiply_fusion.7
  60.4 1.0 bitcast_multiply_fusion.7
  62.9 1.0 bitcast_multiply_fusion.7
  67.8 14.9 %all_gather.44 = bf16[8,4,128]{2,1,0:T(4,128)(2,1)S(1)} all-gather(bf16[1,4,128]{2,1,0:T(4,128)(2,1)S(1)} %copy.224), channel_id=1, replica_groups=mesh['sp_0'=8,'sp_1'=8,'fs'=4,'tp'=2] {'sp_1'}, dimensions={0}, use_global_device_ids=true | all-gather | bytes 9216 | tf_op jit(solution)/shard_map/all_gather | solution.py:38
  83.2 2.5 all-gather.16.cloned.1.call-done
  85.6 2.4 fusion.204
  89.9 11.4 %all_gather.39 = bf16[8,4,128]{2,1,0:T(4,128)(2,1)S(1)} all-gather(bf16[1,4,128]{2,1,0:T(4,128)(2,1)S(1)} %copy.207), channel_id=1, replica_groups=mesh['sp_0'=8,'sp_1'=8,'fs'=4,'tp'=2] {'sp_1'}, dimensions={0}, use_global_device_ids=true | all-gather | bytes 9216 | tf_op jit(solution)/shard_map/all_gather | solution.py:38
  101.8 25.7 %all-gather.14.cloned.1.call-done = bf16[32,128,128]{2,1,0:T(8,128)(2,1)} async-done(((bf16[4,128,128]{2,1,0:T(8,128)(2,1)}), bf16[32,128,128]{2,1,0:T(8,128)(2,1)}) %all-gather.14.cloned.1.call-update) | async-done | bytes 1048592 | tf_op jit(solution)/shard_map/all_gather | solution.py:38
  127.5 2.4 fusion.205
  130.2 2.7 collective-permute-start.3
  133.1 2.6 collective-permute-start
  135.8 0.9 pad_maximum_fusion.1
  136.8 13.6 %all_gather.45 = bf16[8,4,128]{2,1,0:T(4,128)(2,1)S(1)} all-gather(bf16[1,4,128]{2,1,0:T(4,128)(2,1)S(1)} %fusion.313), channel_id=1, replica_groups=mesh['sp_0'=8,'sp_1'=8,'fs'=4,'tp'=2] {'sp_0'}, dimensions={0}, use_global_device_ids=true | all-gather | bytes 9216 | tf_op jit(solution)/shard_map/all_gather | solution.py:38
  151.0 11.0 %all_gather.40 = bf16[8,4,128]{2,1,0:T(4,128)(2,1)S(1)} all-gather(bf16[1,4,128]{2,1,0:T(4,128)(2,1)S(1)} %fusion.312), channel_id=1, replica_groups=mesh['sp_0'=8,'sp_1'=8,'fs'=4,'tp'=2] {'sp_0'}, dimensions={0}, use_global_device_ids=true | all-gather | bytes 9216 | tf_op jit(solution)/shard_map/all_gather | solution.py:38
  163.5 3.2 %collective-permute-start.1 = (bf16[512,256]{1,0:T(8,128)(2,1)S(1)}, bf16[512,256]{1,0:T(8,128)(2,1)S(1)}, u32[]{:S(2)}, u32[]{:S(2)}) collective-permute-start(bf16[512,256]{1,0:T(8,128)(2,1)S(1)} %pad_maximum_fusion.3), channel_id=1, source_target_pairs={{0,16},{8,24},{16,0},{24,8},{32,48},{40,56},{48,32},{56,40},{64,80... | collective-permute-start | bytes 786440 | tf_op jit(solution)/shard_map/ppermute | solution.py:56
  166.8 3.0 %collective-permute-start.4 = (bf16[512,32]{0,1:T(8,128)(2,1)S(1)}, bf16[512,32]{0,1:T(8,128)(2,1)S(1)}, u32[]{:S(2)}, u32[]{:S(2)}) collective-permute-start(bf16[512,32]{0,1:T(8,128)(2,1)S(1)} %pad_maximum_fusion.7), channel_id=1, source_target_pairs={{0,16},{8,24},{16,0},{24,8},{32,48},{40,56},{48,32},{56,40},{64,80... | collective-permute-start | bytes 98312 | tf_op jit(solution)/shard_map/ppermute | solution.py:56
  169.8 5.3 %collective-permute-done.1 = bf16[512,256]{1,0:T(8,128)(2,1)S(1)} collective-permute-done((bf16[512,256]{1,0:T(8,128)(2,1)S(1)}, bf16[512,256]{1,0:T(8,128)(2,1)S(1)}, u32[]{:S(2)}, u32[]{:S(2)}) %collective-permute-start.1) | collective-permute-done | bytes 262176 | tf_op jit(solution)/shard_map/ppermute | solution.py:56
  175.9 4.1 %collective-permute-start.2 = (bf16[1024,256]{1,0:T(8,128)(2,1)}, bf16[1024,256]{1,0:T(8,128)(2,1)}, u32[]{:S(2)}, u32[]{:S(2)}) collective-permute-start(bf16[1024,256]{1,0:T(8,128)(2,1)} %pad_maximum_fusion.2), channel_id=1, source_target_pairs={{0,32},{8,40},{16,48},{24,56},{32,0},{40,8},{48,16},{56,24},{64,96... | collective-permute-start | bytes 1572872 | tf_op jit(solution)/shard_map/ppermute | solution.py:56
  180.2 1.0 copy.227
  181.2 1.0 copy.211
  182.2 5.2 %collective-permute-start.5 = (bf16[1024,32]{0,1:T(8,128)(2,1)S(1)}, bf16[1024,32]{0,1:T(8,128)(2,1)S(1)}, u32[]{:S(2)}, u32[]{:S(2)}) collective-permute-start(bf16[1024,32]{0,1:T(8,128)(2,1)S(1)} %pad_maximum_fusion.6), channel_id=1, source_target_pairs={{0,32},{8,40},{16,48},{24,56},{32,0},{40,8},{48,16},{56,24},{64,96... | collective-permute-start | bytes 196616 | tf_op jit(solution)/shard_map/ppermute | solution.py:56
  187.5 11.3 %collective-permute-done.5 = bf16[1024,32]{0,1:T(8,128)(2,1)S(1)} collective-permute-done((bf16[1024,32]{0,1:T(8,128)(2,1)S(1)}, bf16[1024,32]{0,1:T(8,128)(2,1)S(1)}, u32[]{:S(2)}, u32[]{:S(2)}) %collective-permute-start.5) | collective-permute-done | bytes 65568 | tf_op jit(solution)/shard_map/ppermute | solution.py:56
  198.8 1.1 pad_maximum_fusion
  199.9 15.1 %while.43 = (s32[]{:T(128)}, f32[4,256]{1,0:T(4,128)S(1)}, f32[4,256]{1,0:T(4,128)S(1)}, f32[256,4,64]{0,2,1:T(8,128)S(1)}, bf16[2,1024,256]{2,1,0:T(8,128)(2,1)...) while((s32[]{:T(128)}, f32[4,256]{1,0:T(4,128)S(1)}, ...), condition=%wide.region_15.16_spmd.clone, body=%wide.region_12.15_spmd.clone.sunk | while | flops 614668288 | bytes 34799764 | solution.py:289
  200.5 2.7 bitcast_reduce_fusion.2
  203.3 3.2 %fusion.395 = f32[256,4,64]{0,2,1:T(8,128)S(1)} fusion(f32[4,1024,256]{2,1,0:T(8,128)} %get-tuple-element.580, f32[4,256]{1,0:T(4,128)S(1)} %get-tuple-element.603, bf16[1024,4,128]{0,2,1:T(8,128)(2,1)S(1)} %bitcast.677, f32[256,4,64]{0,2,1:T(8,128)S(1)} %get-tuple-element.595, f32[256,4]{0,1:T(4,128)S(1)} %get-tuple-element.581, pred[]{:T(512)S(6)} %compare.13), kind=kOutput, calls=%fused_computation.81.clone.1 | convolution fusion | flops 137560064 | bytes 5251073 | tf_op jit(solution)/shard_map/while/body/eval_jaxpr/hqk,khv->qhv/dot_general | solution.py:257
  208.1 2.7 bitcast_reduce_fusion.2
  210.9 3.2 %fusion.395 = f32[256,4,64]{0,2,1:T(8,128)S(1)} fusion(f32[4,1024,256]{2,1,0:T(8,128)} %get-tuple-element.580, f32[4,256]{1,0:T(4,128)S(1)} %get-tuple-element.603, bf16[1024,4,128]{0,2,1:T(8,128)(2,1)S(1)} %bitcast.677, f32[256,4,64]{0,2,1:T(8,128)S(1)} %get-tuple-element.595, f32[256,4]{0,1:T(4,128)S(1)} %get-tuple-element.581, pred[]{:T(512)S(6)} %compare.13), kind=kOutput, calls=%fused_computation.81.clone.1 | convolution fusion | flops 137560064 | bytes 5251073 | tf_op jit(solution)/shard_map/while/body/eval_jaxpr/hqk,khv->qhv/dot_general | solution.py:257
  215.8 3.9 %fusion.85 = f32[256,4,128]{0,2,1:T(8,128)S(1)} fusion(f32[256,4,128]{0,2,1:T(8,128)} %copy.227, f32[256,4,128]{2,0,1:T(8,128)} %rev.19, f32[256,4,128]{2,0,1:T(8,128)} %bitcast.699, bf16[8,4,128,128]{3,2,1,0:T(8,128)(2,1)} %all-gather.10.cloned.1.call-done, f32[4,128]{1,0:T(4,128)S(1)} %get-tuple-element.394, f32[4,128]{1,0:T(4,128)S(1)} %get-tuple-element.408, ...), kind=kOutput, calls=%fused_computation.108 | convolution fusion | flops 38010880 | bytes 4229136 | tf_op jit(solution)/shard_map/mcx,cxn->mcn/dot_general | solution.py:209
  220.6 4.0 %multiply_reduce_fusion = (f32[256,4]{0,1:T(4,128)S(1)}, f32[256,4,128]{0,2,1:T(8,128)S(1)}) fusion(f32[256,4,128]{0,2,1:T(8,128)S(1)} %rev.20, f32[256,4,128]{0,2,1:T(8,128)S(1)} %copy-done.15, f32[256,4,128]{2,0,1:T(8,128)S(1)} %copy-done.7, f32[256,4,128]{2,0,1:T(8,128)S(1)} %bitcast.701, bf16[8,4,128,128]{3,2,1,0:T(8,128)(2,1)} %all-gather.8.cloned.1.call-done, ...), kind=kOutput, calls=%fused_computation.126 | convolution fusion | flops 38403072 | bytes 4757520 | tf_op jit(solution)/shard_map/mcx,cxn->mcn/dot_general | solution.py:209
  224.7 37.1 %all-gather.12.cloned.1.call-done = bf16[768,2048]{1,0:T(8,128)(2,1)} async-done(((bf16[768,512]{1,0:T(8,128)(2,1)}), bf16[768,2048]{1,0:T(8,128)(2,1)}) %all-gather.12.cloned.1.call-update) | async-done | bytes 3145744 | tf_op jit(solution)/shard_map/all_gather | solution.py:61
  261.8 1.8 fusion.86
  264.8 5.0 %all_to_all.5 = bf16[2,128,2048]{2,1,0:T(8,128)(2,1)S(1)} all-to-all(bf16[2,128,2048]{2,1,0:T(8,128)(2,1)S(1)} %bitcast.682), channel_id=1, replica_groups=mesh['sp_0'=8,'sp_1'=8,'fs'=4,'tp'=2] {'tp'}, dimensions={0} | all-to-all | bytes 2097152 | tf_op jit(solution)/shard_map/all_to_all | solution.py:75
  269.8 1.1 reduce_sum.41
  (224 shorter events, 29.6 us)
Async XLA Ops:
  7.2 172.9 %copy-start = (bf16[256,1024]{1,0:T(8,128)(2,1)S(1)}, bf16[256,1024]{1,0:T(8,128)(2,1)}, u32[]{:S(2)}) copy-start(bf16[256,1024]{1,0:T(8,128)(2,1)} %param.29) | copy-start | bytes 1572868
  7.2 3.2 %copy-start.17 = (bf16[1,256,512]{2,1,0:T(8,128)(2,1)S(1)}, bf16[1,256,512]{2,1,0:T(8,128)(2,1)}, u32[]{:S(2)}) copy-start(bf16[1,256,512]{2,1,0:T(8,128)(2,1)} %param.21) | copy-start | bytes 786436
  7.2 3.4 %copy-start.20 = (f32[1,256,4]{1,2,0:T(4,128)S(1)}, f32[1,256,4]{1,2,0:T(4,128)}, u32[]{:S(2)}) copy-start(f32[1,256,4]{1,2,0:T(4,128)} %param.23) | copy-start | bytes 12292
  7.2 78.4 %all-gather.16.cloned.1.call-start = ((), (), s32[]{:S(2)}) async-start(), calls=%async_computation.5 | async-start | bytes 1179648 | tf_op jit(solution)/shard_map/all_gather | solution.py:38
  10.5 13.5 %copy-start.3 = (bf16[1,256,512]{1,2,0:T(8,128)(2,1)}, bf16[1,256,512]{1,2,0:T(8,128)(2,1)S(1)}, u32[]{:S(2)}) copy-start(bf16[1,256,512]{1,2,0:T(8,128)(2,1)S(1)} %copy.197) | copy-start | bytes 786436
  21.4 7.6 %copy-start.6 = (f32[256,4,128]{2,0,1:T(8,128)}, f32[256,4,128]{2,0,1:T(8,128)S(1)}, u32[]{:S(2)}) copy-start(f32[256,4,128]{2,0,1:T(8,128)S(1)} %copy.209) | copy-start | bytes 1572868
  43.4 3.8 %copy-start.4 = (bf16[1,256,512]{1,2,0:T(8,128)(2,1)S(1)}, bf16[1,256,512]{1,2,0:T(8,128)(2,1)}, u32[]{:S(2)}) copy-start(bf16[1,256,512]{1,2,0:T(8,128)(2,1)} %copy-done.3) | copy-start | bytes 786436
  44.1 83.4 %all-gather.14.cloned.1.call-start = ((), (), s32[]{:S(2)}) async-start(), calls=%async_computation.4 | async-start | bytes 1179648 | tf_op jit(solution)/shard_map/all_gather | solution.py:38
  45.1 2.4 copy-start.8
  66.0 149.7 %all-gather.10.cloned.1.call-start = ((), (), s32[]{:S(2)}) async-start(), calls=%async_computation.2 | async-start | bytes 1179648 | tf_op jit(solution)/shard_map/all_gather | solution.py:38
  66.3 21.9 %copy-start.5 = (f32[128,4,256]{2,0,1:T(8,128)S(1)}, f32[128,4,256]{2,0,1:T(8,128)}, u32[]{:S(2)}) copy-start(f32[128,4,256]{2,0,1:T(8,128)} %get-tuple-element.369) | copy-start | bytes 1572868
  66.9 0.8 copy-start.11
  88.1 132.4 %all-gather.8.cloned.1.call-start = ((), (), s32[]{:S(2)}) async-start(), calls=%async_computation.1 | async-start | bytes 1179648 | tf_op jit(solution)/shard_map/all_gather | solution.py:38
  88.4 41.7 %copy-start.21 = (bf16[1,256,32]{1,2,0:T(8,128)(2,1)S(1)}, bf16[1,256,32]{1,2,0:T(8,128)(2,1)}, u32[]{:S(2)}) copy-start(bf16[1,256,32]{1,2,0:T(8,128)(2,1)} %param.27) | copy-start | bytes 49156
  88.8 44.1 %copy-start.16 = (bf16[1,256,256]{2,1,0:T(8,128)(2,1)S(1)}, bf16[1,256,256]{2,1,0:T(8,128)(2,1)}, u32[]{:S(2)}) copy-start(bf16[1,256,256]{2,1,0:T(8,128)(2,1)} %param.26) | copy-start | bytes 393220
  88.8 44.2 %copy-start.31 = (f32[256]{0:T(256)S(1)}, f32[256]{0:T(256)}, u32[]{:S(2)}) copy-start(f32[256]{0:T(256)} %param.28) | copy-start | bytes 3076
  88.8 47.0 %copy-start.14 = (bf16[512,512]{1,0:T(8,128)(2,1)S(1)}, bf16[512,512]{1,0:T(8,128)(2,1)}, u32[]{:S(2)}) copy-start(bf16[512,512]{1,0:T(8,128)(2,1)} %param.30) | copy-start | bytes 1572868
  88.8 47.0 %copy-start.18 = (bf16[256,512]{1,0:T(8,128)(2,1)S(1)}, bf16[256,512]{1,0:T(8,128)(2,1)}, u32[]{:S(2)}) copy-start(bf16[256,512]{1,0:T(8,128)(2,1)} %param.31) | copy-start | bytes 786436
  89.0 0.8 copy-start.12
  127.5 35.2 %copy-start.19 = (bf16[1,256,384]{2,1,0:T(8,128)(2,1)S(1)}, bf16[1,256,384]{2,1,0:T(8,128)(2,1)}, u32[]{:S(2)}) copy-start(bf16[1,256,384]{2,1,0:T(8,128)(2,1)} %param.25) | copy-start | bytes 589828
  129.9 131.9 %all-gather.12.cloned.1.call-start = ((), (), s32[]{:S(2)}) async-start(), calls=%async_computation.3 | async-start | bytes 3932160 | tf_op jit(solution)/shard_map/all_gather | solution.py:61
  130.2 36.6 %collective-permute-start.3 = (bf16[256,32]{0,1:T(8,128)(2,1)S(1)}, bf16[256,32]{0,1:T(8,128)(2,1)S(1)}, u32[]{:S(2)}, u32[]{:S(2)}) collective-permute-start(bf16[256,32]{0,1:T(8,128)(2,1)S(1)} %pad_maximum_fusion.8), channel_id=1, source_target_pairs={{0,8},{8,0},{16,24},{24,16},{32,40},{40,32},{48,56},{56,48},{64,72... | collective-permute-start | bytes 49160 | tf_op jit(solution)/shard_map/ppermute | solution.py:56
  133.1 30.4 %collective-permute-start = (bf16[256,256]{1,0:T(8,128)(2,1)S(1)}, bf16[256,256]{1,0:T(8,128)(2,1)S(1)}, u32[]{:S(2)}, u32[]{:S(2)}) collective-permute-start(bf16[256,256]{1,0:T(8,128)(2,1)S(1)} %fusion.155), channel_id=1, source_target_pairs={{0,8},{8,0},{16,24},{24,16},{32,40},{40,32},{48,56},{56,48},{64,72... | collective-permute-start | bytes 393224 | tf_op jit(solution)/shard_map/ppermute | solution.py:56
  136.7 43.5 %copy-start.9 = (f32[4,64,4,128]{3,1,0,2:T(8,128)S(1)}, f32[4,64,4,128]{3,1,0,2:T(8,128)}, u32[]{:S(2)}) copy-start(f32[4,64,4,128]{3,1,0,2:T(8,128)} %get-tuple-element.134) | copy-start | bytes 1572868
  162.7 18.5 %copy-start.10 = (f32[4,64,4,128]{3,1,0,2:T(8,128)S(1)}, f32[4,64,4,128]{3,1,0,2:T(8,128)}, u32[]{:S(2)}) copy-start(f32[4,64,4,128]{3,1,0,2:T(8,128)} %get-tuple-element.132) | copy-start | bytes 1572868
  163.5 11.6 %collective-permute-start.1 = (bf16[512,256]{1,0:T(8,128)(2,1)S(1)}, bf16[512,256]{1,0:T(8,128)(2,1)S(1)}, u32[]{:S(2)}, u32[]{:S(2)}) collective-permute-start(bf16[512,256]{1,0:T(8,128)(2,1)S(1)} %pad_maximum_fusion.3), channel_id=1, source_target_pairs={{0,16},{8,24},{16,0},{24,8},{32,48},{40,56},{48,32},{56,40},{64,80... | collective-permute-start | bytes 786440 | tf_op jit(solution)/shard_map/ppermute | solution.py:56
  166.8 15.4 %collective-permute-start.4 = (bf16[512,32]{0,1:T(8,128)(2,1)S(1)}, bf16[512,32]{0,1:T(8,128)(2,1)S(1)}, u32[]{:S(2)}, u32[]{:S(2)}) collective-permute-start(bf16[512,32]{0,1:T(8,128)(2,1)S(1)} %pad_maximum_fusion.7), channel_id=1, source_target_pairs={{0,16},{8,24},{16,0},{24,8},{32,48},{40,56},{48,32},{56,40},{64,80... | collective-permute-start | bytes 98312 | tf_op jit(solution)/shard_map/ppermute | solution.py:56
  175.9 22.9 %collective-permute-start.2 = (bf16[1024,256]{1,0:T(8,128)(2,1)}, bf16[1024,256]{1,0:T(8,128)(2,1)}, u32[]{:S(2)}, u32[]{:S(2)}) collective-permute-start(bf16[1024,256]{1,0:T(8,128)(2,1)} %pad_maximum_fusion.2), channel_id=1, source_target_pairs={{0,32},{8,40},{16,48},{24,56},{32,0},{40,8},{48,16},{56,24},{64,96... | collective-permute-start | bytes 1572872 | tf_op jit(solution)/shard_map/ppermute | solution.py:56
  182.2 16.6 %collective-permute-start.5 = (bf16[1024,32]{0,1:T(8,128)(2,1)S(1)}, bf16[1024,32]{0,1:T(8,128)(2,1)S(1)}, u32[]{:S(2)}, u32[]{:S(2)}) collective-permute-start(bf16[1024,32]{0,1:T(8,128)(2,1)S(1)} %pad_maximum_fusion.6), channel_id=1, source_target_pairs={{0,32},{8,40},{16,48},{24,56},{32,0},{40,8},{48,16},{56,24},{64,96... | collective-permute-start | bytes 196616 | tf_op jit(solution)/shard_map/ppermute | solution.py:56
  203.3 3.5 %copy-start.1 = (f32[4,1024,256]{2,1,0:T(8,128)S(1)}, f32[4,1024,256]{2,1,0:T(8,128)}, u32[]{:S(2)}) copy-start(f32[4,1024,256]{2,1,0:T(8,128)} %get-tuple-element.580) | copy-start | bytes 12582916 | tf_op jit(solution)/shard_map/while
  210.9 3.5 %copy-start.1 = (f32[4,1024,256]{2,1,0:T(8,128)S(1)}, f32[4,1024,256]{2,1,0:T(8,128)}, u32[]{:S(2)}) copy-start(f32[4,1024,256]{2,1,0:T(8,128)} %get-tuple-element.580) | copy-start | bytes 12582916 | tf_op jit(solution)/shard_map/while
  215.7 4.7 %copy-start.7 = (f32[256,4,128]{2,0,1:T(8,128)S(1)}, f32[256,4,128]{2,0,1:T(8,128)}, u32[]{:S(2)}) copy-start(f32[256,4,128]{2,0,1:T(8,128)} %copy-done.6) | copy-start | bytes 1572868
  215.7 4.7 %copy-start.13 = (f32[128,4,2,128]{0,3,2,1:T(8,128)S(1)}, f32[128,4,2,128]{0,3,2,1:T(8,128)}, u32[]{:S(2)}) copy-start(f32[128,4,2,128]{0,3,2,1:T(8,128)} %copy-done.12) | copy-start | bytes 1572868
  215.7 4.7 %copy-start.15 = (f32[256,4,128]{0,2,1:T(8,128)S(1)}, f32[256,4,128]{0,2,1:T(8,128)}, u32[]{:S(2)}) copy-start(f32[256,4,128]{0,2,1:T(8,128)} %copy.211) | copy-start | bytes 1572868
  215.7 4.7 %copy-start.23 = (f32[4,128]{1,0:T(4,128)S(1)}, f32[4,128]{1,0:T(4,128)}, u32[]{:S(2)}) copy-start(f32[4,128]{1,0:T(4,128)} %get-tuple-element.377) | copy-start | bytes 6148
  215.7 4.7 %copy-start.24 = (f32[4,128]{1,0:T(4,128)S(1)}, f32[4,128]{1,0:T(4,128)}, u32[]{:S(2)}) copy-start(f32[4,128]{1,0:T(4,128)} %get-tuple-element.379) | copy-start | bytes 6148
  215.8 4.7 %copy-start.25 = (f32[4,128]{1,0:T(4,128)S(1)}, f32[4,128]{1,0:T(4,128)}, u32[]{:S(2)}) copy-start(f32[4,128]{1,0:T(4,128)} %get-tuple-element.380) | copy-start | bytes 6148
  215.8 4.7 %copy-start.26 = (f32[4,128]{1,0:T(4,128)S(1)}, f32[4,128]{1,0:T(4,128)}, u32[]{:S(2)}) copy-start(f32[4,128]{1,0:T(4,128)} %get-tuple-element.381) | copy-start | bytes 6148
  215.8 4.7 %copy-start.27 = (f32[4,128]{1,0:T(4,128)S(1)}, f32[4,128]{1,0:T(4,128)}, u32[]{:S(2)}) copy-start(f32[4,128]{1,0:T(4,128)} %get-tuple-element.382) | copy-start | bytes 6148
  215.8 4.7 %copy-start.28 = (f32[4,128]{1,0:T(4,128)S(1)}, f32[4,128]{1,0:T(4,128)}, u32[]{:S(2)}) copy-start(f32[4,128]{1,0:T(4,128)} %get-tuple-element.383) | copy-start | bytes 6148
  215.8 4.7 %copy-start.29 = (f32[4,128]{1,0:T(4,128)S(1)}, f32[4,128]{1,0:T(4,128)}, u32[]{:S(2)}) copy-start(f32[4,128]{1,0:T(4,128)} %get-tuple-element.384) | copy-start | bytes 6148
  215.8 4.7 %copy-start.30 = (f32[4,128]{1,0:T(4,128)S(1)}, f32[4,128]{1,0:T(4,128)}, u32[]{:S(2)}) copy-start(f32[4,128]{1,0:T(4,128)} %get-tuple-element.385) | copy-start | bytes 6148
  220.6 4.0 %copy-start.22 = (f32[512]{0:T(512)S(1)}, f32[512]{0:T(512)}, u32[]{:S(2)}) copy-start(f32[512]{0:T(512)} %param.24) | copy-start | bytes 6148
  261.8 2.2 copy-start.2
Sparse Core Ops, SparseCore 0:
  44.2 41.4 all-gather.15
  87.7 39.6 all-gather.13
  129.6 41.0 all-gather.9
  172.6 39.4 all-gather.7
  214.0 47.7 all-gather.11
where the time goes:
time: 279 us; the launch traced here: 277 us
  waiting for transfers between devices  82 us (29%)
  blocking collectives  55.9 us (20%)
  local copies, waits for them, and re-layouts  36.9 us (13%)
  matrix products  34.1 us (12%)
  other arithmetic  32.2 us (12%)
  starting transfers between devices  21 us (8%)
  between operations  14.8 us (5%)
    all_gather x4, blocking collectives, carried_in(): lax.all_gather(part.astype(kind), axis)  50.9 us
    all_gather x1, waiting for transfers between devices, sent_together(): lax.all_gather(both, axis, axis=dim, tiled=True)  37.1 us
    all_gather x4, waiting for transfers between devices, carried_in(): lax.all_gather(part.astype(kind), axis)  28.2 us
    ppermute x6, starting transfers between devices, from_partner(): return lax.ppermute(value, axis, pairs)  20.8 us
    ppermute x6, waiting for transfers between devices, from_partner(): return lax.ppermute(value, axis, pairs)  16.7 us
    rev x7, local copies, waits for them, and re-layouts, local(): sorted_rows = [jnp.flip(member, axis=0) for member in sorted_rows]  13.5 us
    mul x8, other arithmetic, advance(): key_decayed = key_tile * jnp.exp(-inner_block_term)  8.49 us
    dot_general x2, matrix products, local(): jnp.einsum('mcx,cxn->mcn', sorted_rows[0] * jnp.exp(running_state), arriv...  7.83 us
  transfers between devices with their start and end apart: 11, of which 5 were waited for; matrix products, arithmetic and copies ran while one was open for 22% of the time, Pallas kernels for 0%

commit v1 on v0

v1 whole, which is shorter than its diff:
```python
import numpy as np

import jax
import jax.numpy as jnp
from jax import lax
from jax.experimental import pallas as pl
from jax.experimental.pallas import tpu as pltpu
from jax.sharding import Mesh
from jax.sharding import PartitionSpec as P

DK = 128
HEADS = 4
NOPE = 64
ROPE = 32
RANK = 256
BLOCK = 64
TOK = 256
HALF = 128
SEQ_DEV = 8
STATE_ROWS = 144
KV_ROWS = 288
CHUNK_ROWS = STATE_ROWS + KV_ROWS
SP = ("sp_0", "sp_1")
SP_TP = ("sp_0", "sp_1", "tp")
EPS = 1e-06
ROPE_BASE = 10000.0
SCALE = (NOPE + ROPE) ** (-0.5)
LOG2E = 1.4426950408889634

f32 = jnp.float32
bf16 = jnp.bfloat16
NT = (((1,), (1,)), ((), ()))
TN = (((0,), (0,)), ((), ()))


def dot(a, b, dims=(((1,), (0,)), ((), ()))):
    return lax.dot_general(a, b, dims, preferred_element_type=f32)


def iota2(shape, axis):
    return lax.broadcasted_iota(jnp.int32, shape, axis)


def exact_sum(selector, values):
    high = values.astype(bf16)
    rest = values - high.astype(f32)
    middle = rest.astype(bf16)
    low = (rest - middle.astype(f32)).astype(bf16)
    return dot(selector, high) + dot(selector, middle) + dot(selector, low)


def gate(logit, floor, extra):
    keyed = (1.0 - floor) * logit
    return keyed, jnp.log(1.0 - keyed) + extra


def head_extra(extra_ref, first, count):
    return jnp.concatenate(
        [
            jnp.broadcast_to(extra_ref[:, h : h + 1], (TOK, DK))
            for h in range(first, first + count)
        ],
        axis=1,
    )


def rotated(x, cos_table, sin_table):
    lane = iota2(x.shape, 1)
    partner = jnp.where(lane < NOPE + ROPE // 2, pltpu.roll(x, 128 - 16, 1), pltpu.roll(x, 16, 1))
    return x * cos_table + partner * sin_table


def send_kernel(
    tp_ref, logit_ref, value_ref, floor_ref, extra_ref, lat_ref, gain_ref, key_ref, cos_ref, sin_ref, out_ref
):
    rows = iota2((TOK, TOK), 0)
    cols = iota2((TOK, TOK), 1)
    after = (cols > rows).astype(f32).astype(bf16)
    before = (cols < rows).astype(f32).astype(bf16)
    for pair in range(HEADS // 2):
        lanes = slice(pair * 2 * DK, (pair + 1) * 2 * DK)
        closed = jax.nn.sigmoid(-logit_ref[:, lanes].astype(f32))
        extra = head_extra(extra_ref, 2 * pair, 2)
        for d in range(2):
            keyed, decay = gate(closed, floor_ref[d : d + 1, lanes], extra)
            left = exact_sum(after if d == 0 else before, decay)
            edge = 0 if d == 0 else TOK - 1
            total = jnp.exp(left[edge : edge + 1] + decay[edge : edge + 1])
            weighted = (keyed * jnp.exp(left)).astype(bf16)
            for s in range(2):
                h = 2 * pair + s
                state = dot(
                    value_ref[:, h * DK : (h + 1) * DK], weighted[:, s * DK : (s + 1) * DK], TN
                )
                out_ref[d * HEADS + h, 0:DK, :] = state.astype(bf16)
                out_ref[d * HEADS + h, DK:STATE_ROWS, :] = jnp.broadcast_to(
                    total[:, s * DK : (s + 1) * DK], (STATE_ROWS - DK, DK)
                ).astype(bf16)
    mine = pl.ds(pl.multiple_of(tp_ref[0] * HALF, HALF), HALF)
    wide = lat_ref[mine, :].astype(f32)
    mean = jnp.sum(wide * wide, axis=1, keepdims=True) * (1.0 / RANK)
    normed = (wide * lax.rsqrt(mean + EPS) * gain_ref[...]).astype(bf16)
    turned = rotated(key_ref[mine, :].astype(f32), cos_ref[mine, :], sin_ref[mine, :])
    lane = iota2((32, 128), 1)
    packed = jnp.zeros((32, 128), f32)
    for g in range(4):
        piece = pltpu.roll(turned[32 * g : 32 * g + 32], (32 * g - NOPE) % 128, 1)
        packed = jnp.where((lane >= 32 * g) & (lane < 32 * g + 32), piece, packed)
    packed = packed.astype(bf16)
    for q in range(SEQ_DEV):
        out_ref[q, STATE_ROWS : STATE_ROWS + 128, :] = normed[:, :128]
        out_ref[q, STATE_ROWS + 128 : STATE_ROWS + 256, :] = normed[:, 128:]
        out_ref[q, STATE_ROWS + 256 : CHUNK_ROWS, :] = packed


def local_kernel(query_ref, logit_ref, value_ref, floor_ref, extra_ref, out_ref, damped_ref):
    rows = iota2((TOK, TOK), 0)
    cols = iota2((TOK, TOK), 1)
    same = (rows // BLOCK) == (cols // BLOCK)
    lower = same & (cols <= rows)
    upper = same & (cols >= rows)
    blocks = TOK // BLOCK
    for h in range(HEADS):
        lanes = slice(h * DK, (h + 1) * DK)
        closed = jax.nn.sigmoid(-logit_ref[:, lanes].astype(f32))
        extra = head_extra(extra_ref, h, 1)
        query = query_ref[:, lanes].astype(f32)
        value = value_ref[:, lanes]
        outs = [None] * blocks
        inner_sum = jnp.zeros((TOK, DK), f32)
        for d in range(2):
            seen = lower if d == 0 else upper
            keyed, decay = gate(closed, floor_ref[d : d + 1, lanes], extra)
            within = exact_sum(seen.astype(f32).astype(bf16), decay)
            damped = query * jnp.exp(within)
            grown = (keyed * jnp.exp(-within)).astype(bf16)
            damped16 = damped.astype(bf16)
            scores = jnp.where(seen, dot(damped16, grown, NT), 0.0).astype(bf16)
            inner_sum = inner_sum + dot(scores, value)
            state = None
            offset = jnp.zeros((1, DK), f32)
            for b in range(blocks) if d == 0 else reversed(range(blocks)):
                at = slice(b * BLOCK, (b + 1) * BLOCK)
                edge = (b + 1) * BLOCK - 1 if d == 0 else b * BLOCK
                total = within[edge : edge + 1]
                damped_ref[d, at, lanes] = (damped[at] * jnp.exp(offset)).astype(bf16)
                if state is not None:
                    cross = dot(damped16[at], state.astype(bf16), NT)
                    outs[b] = cross if outs[b] is None else outs[b] + cross
                offset = offset + total
                if b == (blocks - 1 if d == 0 else 0):
                    continue
                weighted = (keyed[at] * jnp.exp(total - within[at])).astype(bf16)
                added = dot(value[at], weighted, TN)
                state = added if state is None else state * jnp.exp(total) + added
        for b in range(blocks):
            at = slice(b * BLOCK, (b + 1) * BLOCK)
            out_ref[at, lanes] = inner_sum[at] if outs[b] is None else inner_sum[at] + outs[b]


def scan_kernel(dir_ref, got_ref, out_ref):
    d = dir_ref[0]
    carried = jnp.zeros((DK, DK), f32)
    for k in range(SEQ_DEV):
        j = jnp.where(d == 0, k, SEQ_DEV - 1 - k)
        out_ref[j] = carried.astype(bf16)
        if k < SEQ_DEV - 1:
            decay = got_ref[j, DK:STATE_ROWS, :][0:1].astype(f32)
            carried = carried * decay + got_ref[j, 0:DK, :].astype(f32)


def attend_kernel(
    tp_ref, query_ref, mine_ref, other_ref, up_ref, cos_ref, sin_ref, out_ref, lw_ref, ex_ref, rope_ref
):
    up = up_ref[:, pl.ds(pl.multiple_of(tp_ref[0] * HEADS * 128, HEADS * 128), HEADS * 128)]
    lane32 = iota2((32, 128), 1)
    in_rope = (lane32 >= NOPE) & (lane32 < NOPE + ROPE)
    for c in range(2):
        for j in range(SEQ_DEV):
            ref, base = (mine_ref, STATE_ROWS) if c == 0 else (other_ref, 0)
            lat = jnp.concatenate(
                [ref[j, base : base + 128, :], ref[j, base + 128 : base + 256, :]], axis=1
            )
            at = (c * SEQ_DEV + j) * 128
            ex_ref[at : at + 128, :] = dot(lat, up).astype(bf16)
            packed = ref[j, base + 256 : base + 288, :].astype(f32)
            for g in range(4):
                piece = pltpu.roll(packed, (NOPE - 32 * g) % 128, 1)
                rope_ref[at + 32 * g : at + 32 * g + 32, :] = jnp.where(in_rope, piece, 0.0).astype(bf16)
    lane = iota2((TOK, 128), 1)
    q_blocks = [query_ref[:, 128 * i : 128 * i + 128].astype(f32) for i in range(3)]
    key_lane = iota2((SEQ_DEV * TOK, 128), 1)
    for h in range(HEADS):
        lanes = slice(h * 128, (h + 1) * 128)
        if h == 0:
            q = q_blocks[0]
        elif h == 1:
            q = jnp.where(lane < 32, pltpu.roll(q_blocks[0], 32, 1), pltpu.roll(q_blocks[1], 32, 1))
        elif h == 2:
            q = jnp.where(lane < 64, pltpu.roll(q_blocks[1], 64, 1), pltpu.roll(q_blocks[2], 64, 1))
        else:
            q = pltpu.roll(q_blocks[2], 96, 1)
        q = rotated(q, cos_ref[...], sin_ref[...]).astype(bf16)
        ex = ex_ref[:, lanes]
        keys = jnp.where(key_lane < NOPE, ex, rope_ref[...])
        scores = dot(q, keys, NT)
        peak = jnp.max(scores, axis=1, keepdims=True)
        weights = jnp.exp2((scores - peak) * (SCALE * LOG2E))
        total = jnp.sum(weights, axis=1, keepdims=True)
        mixed = dot(weights.astype(bf16), ex) / total
        lw_ref[:, h : h + 1] = peak * SCALE + jnp.log(total)
        if h % 2 == 0:
            kept = pltpu.roll(mixed, 64, 1)
        else:
            out_ref[:, (h // 2) * 128 : (h // 2) * 128 + 128] = jnp.where(
                lane < 64, kept, mixed
            ).astype(bf16)


def finish_kernel(
    idx_ref, local_ref, damped_ref, state_ref, gain_ref, att_ref,
    own_ref, left_ref, right_ref, far_a_ref, far_b_ref, send_ref, keep_ref, act_ref,
):
    tp = idx_ref[0]
    for part in range(2):
        start = jnp.where(tp == part, HALF, 0)
        at = pl.ds(pl.multiple_of(start, HALF), HALF)
        to = slice(part * HALF, (part + 1) * HALF)
        for h in range(HEADS):
            lanes = slice(h * DK, (h + 1) * DK)
            o = (
                local_ref[at, lanes]
                + dot(damped_ref[0, at, lanes], state_ref[h], NT)
                + dot(damped_ref[1, at, lanes], state_ref[HEADS + h], NT)
            )
            mean = jnp.sum(o * o, axis=1, keepdims=True) * (1.0 / DK)
            act_ref[to, lanes] = (o * lax.rsqrt(mean + EPS) * gain_ref[:, lanes]).astype(bf16)
        act_ref[to, HEADS * DK :] = att_ref[at, :]
    act = act_ref[...]
    for i in range(4):
        if i < 3:
            got = dot(act, (own_ref, left_ref, right_ref)[i][...])
        else:
            got = dot(act[:, :384], far_a_ref[...]) + dot(act[:, 384:], far_b_ref[...])
        got = got.astype(bf16)
        lanes = pl.ds(pl.multiple_of(idx_ref[1 + i] * 512, 512), 512)
        send_ref[:, lanes] = got[:HALF]
        keep_ref[:, lanes] = got[HALF:]


def call(kernel, outs, *args, scratch=(), flops=0, name=None, smem=0):
    specs = [
        pl.BlockSpec(memory_space=pltpu.SMEM) if i < smem else pl.BlockSpec(memory_space=pltpu.VMEM)
        for i in range(len(args))
    ]
    single = not isinstance(outs, tuple)
    return pl.pallas_call(
        kernel,
        out_shape=outs,
        in_specs=specs,
        out_specs=pl.BlockSpec(memory_space=pltpu.VMEM)
        if single
        else tuple(pl.BlockSpec(memory_space=pltpu.VMEM) for _ in outs),
        scratch_shapes=list(scratch),
        cost_estimate=pl.CostEstimate(flops=flops, bytes_accessed=1 << 20, transcendentals=0),
        name=name,
    )(*args)


def shape(dims, dtype):
    return jax.ShapeDtypeStruct(dims, dtype)


def ring(n, step):
    return [(i, (i + step) % n) for i in range(n)]


def exchange(value):
    return lax.all_to_all(value, "sp_1", split_axis=0, concat_axis=0, tiled=True)


def local(
    recurrent_query,
    forget_logits,
    recurrent_value,
    forget_floor,
    extra_log_decay,
    recurrent_norm_gain,
    attention_query,
    latent,
    rotary_key,
    latent_norm_gain,
    latent_up_weight,
    recurrent_output_weight,
    attention_output_weight,
):
    place = lax.axis_index("sp_1")
    column = lax.axis_index("fs")
    tp = lax.axis_index("tp")
    lane = np.arange(128)
    inverse = np.power(
        np.float32(ROPE_BASE), (-(lane % 16).astype(np.float32) / np.float32(16)), dtype=np.float32
    )
    position = (place * TOK + jnp.arange(TOK)).astype(f32)
    angle = position[:, None] * inverse[None, :]
    first = (lane >= NOPE) & (lane < NOPE + ROPE // 2)
    second = (lane >= NOPE + ROPE // 2) & (lane < NOPE + ROPE)
    cos_table = jnp.where(first | second, jnp.cos(angle), (lane < NOPE).astype(np.float32))
    sin_table = jnp.sin(angle) * (second.astype(np.float32) - first.astype(np.float32))

    tp_at = tp.astype(jnp.int32).reshape(1)
    logits, values, extra = forget_logits[0], recurrent_value[0], extra_log_decay[0]
    padded_key = jnp.pad(rotary_key[0], ((0, 0), (NOPE, 128 - NOPE - ROPE)))

    sent = call(
        send_kernel,
        shape((SEQ_DEV, CHUNK_ROWS, DK), bf16),
        tp_at, logits, values, forget_floor, extra, latent[0], latent_norm_gain.reshape(1, RANK),
        padded_key, cos_table, sin_table,
        flops=1 << 29, name="send", smem=1,
    )
    got = exchange(sent)

    weights = jnp.concatenate([recurrent_output_weight, attention_output_weight], axis=0)
    from_left = lax.ppermute(weights, "fs", ring(4, 1))
    from_right = lax.ppermute(weights, "fs", ring(4, -1))
    far_a = lax.ppermute(from_left[:384], "fs", ring(4, 1))
    far_b = lax.ppermute(from_right[384:], "fs", ring(4, -1))

    local_out, damped = call(
        local_kernel,
        (shape((TOK, HEADS * DK), f32), shape((2, TOK, HEADS * DK), bf16)),
        recurrent_query[0], logits, values, forget_floor, extra,
        flops=1 << 30, name="local",
    )

    scanned = call(
        scan_kernel,
        shape((SEQ_DEV, DK, DK), bf16),
        (place // HEADS).astype(jnp.int32).reshape(1), got,
        flops=1 << 26, name="scan", smem=1,
    )
    states = exchange(scanned)

    other = lax.ppermute(got[:, STATE_ROWS:], "tp", [(0, 1), (1, 0)])
    attended, log_weight = call(
        attend_kernel,
        (shape((TOK, HEADS * 64), bf16), shape((TOK, HEADS), f32)),
        tp_at, attention_query[0], got, other, latent_up_weight, cos_table, sin_table,
        scratch=(pltpu.VMEM((SEQ_DEV * TOK, HEADS * 128), bf16), pltpu.VMEM((SEQ_DEV * TOK, 128), bf16)),
        flops=1 << 31, name="attend", smem=1,
    )

    index = jnp.stack([tp, column, (column + 3) % 4, (column + 1) % 4, (column + 2) % 4]).astype(jnp.int32)
    send, keep = call(
        finish_kernel,
        (shape((HALF, 2048), bf16), shape((HALF, 2048), bf16)),
        index, local_out, damped, states, recurrent_norm_gain.reshape(1, HEADS * DK), attended,
        weights, from_left, from_right, far_a, far_b,
        scratch=(pltpu.VMEM((TOK, 768), bf16),),
        flops=1 << 30, name="finish", smem=1,
    )
    arrived = lax.ppermute(send, "tp", [(0, 1), (1, 0)])
    mixed = (keep.astype(f32) + arrived.astype(f32)).astype(bf16)
    return mixed[None], log_weight[None]


def solution(mesh):
    torus = Mesh(
        mesh.devices.reshape(8, 8, mesh.shape["fs"], mesh.shape["tp"]), ("sp_0", "sp_1", "fs", "tp")
    )
    in_specs = (
        P("fs", SP, "tp"),
        P("fs", SP, "tp"),
        P("fs", SP, "tp"),
        P(None, "tp"),
        P("fs", SP, "tp"),
        P("tp"),
        P("fs", SP, "tp"),
        P("fs", SP, None),
        P("fs", SP, None),
        P(),
        P(),
        P("tp", "fs"),
        P("tp", "fs"),
    )
    out_specs = (P("fs", SP_TP, None), P("fs", SP, "tp"))
    return jax.shard_map(local, mesh=torus, in_specs=in_specs, out_specs=out_specs, check_vma=False)
```

time: 279 us -> 85.7 us (0.31)
  waiting for transfers between devices: 82 us -> 17.1 us
  blocking collectives: 55.9 us -> 0 us
  matrix products: 34.1 us -> 0 us
  other arithmetic: 32.2 us -> 3.24 us
  local copies, waits for them, and re-layouts: 36.9 us -> 8.21 us
  Pallas kernels: 0 us -> 24.3 us
  between operations: 14.8 us -> 0.92 us
  starting transfers between devices: 21 us -> 31.3 us
    all_gather x5 -> x0, waiting for transfers between devices: 65.3 us -> none  [the longest x1 37.1 us: sent_together(): lax.all_gather(both, axis, axis=dim, tiled=True)]
    all_gather x4 -> x0, blocking collectives: 50.9 us -> none  [carried_in(): lax.all_gather(part.astype(kind), axis)]
    dot_general x34 -> x0, matrix products: 34.1 us -> none  [the longest x2 7.83 us: local(): jnp.einsum('mcx,cxn->mcn', sorted_rows[0] * jnp.exp(running_state), arriv...]
    pallas_call x0 -> x5, Pallas kernels: none -> 24.3 us  [call(): pl.pallas_call(kernel, out_shape=outs, in_specs=specs, out_specs=pl.Block...]
    all_to_all x0 -> x2, waiting for transfers between devices: none -> 16.1 us  [exchange(): lax.all_to_all(value, 'sp_1', split_axis=0, concat_axis=0, tiled=True)]
    ppermute x6, waiting for transfers between devices: 16.7 us -> 1.05 us  [the longest x1 1.04 us: local(): arrived = lax.ppermute(send, 'tp', [(0, 1), (1, 0)])]
    rev x8 -> x0, local copies, waits for them, and re-layouts: 14.2 us -> none  [the longest x7 13.5 us: local(): sorted_rows = [jnp.flip(member, axis=0) for member in sorted_rows]]
    all_to_all x0 -> x2, starting transfers between devices: none -> 11.2 us  [exchange(): lax.all_to_all(value, 'sp_1', split_axis=0, concat_axis=0, tiled=True)]
  transfers between devices with their start and end apart: 11 -> 8, of which waited for: 5 -> 2; matrix products, arithmetic and copies ran while one was open for 22% -> 5% of each run, Pallas kernels for 0% -> 18%
where the time goes in v1:
time: 85.7 us; the launch traced here: 85.1 us
  starting transfers between devices  31.3 us (37%)
  Pallas kernels  24.3 us (28%)
  waiting for transfers between devices  17.1 us (20%)
  local copies, waits for them, and re-layouts  8.21 us (10%)
  other arithmetic  3.24 us (4%)
  between operations  0.92 us (1%)
    pallas_call x5, Pallas kernels, call(): pl.pallas_call(kernel, out_shape=outs, in_specs=specs, out_specs=pl.Block...  24.3 us
    all_to_all x2, waiting for transfers between devices, exchange(): lax.all_to_all(value, 'sp_1', split_axis=0, concat_axis=0, tiled=True)  16.1 us
    all_to_all x2, starting transfers between devices, exchange(): lax.all_to_all(value, 'sp_1', split_axis=0, concat_axis=0, tiled=True)  11.2 us
    ppermute x1, starting transfers between devices, local(): other = lax.ppermute(got[:, STATE_ROWS:], 'tp', [(0, 1), (1, 0)])  4.51 us
    unnamed x36, local copies, waits for them, and re-layouts  4.23 us
    ppermute x1, starting transfers between devices, local(): far_b = lax.ppermute(from_right[384:], 'fs', ring(4, -1))  3.55 us
    ppermute x1, starting transfers between devices, local(): from_right = lax.ppermute(weights, 'fs', ring(4, -1))  3.37 us
    ppermute x1, starting transfers between devices, local(): from_left = lax.ppermute(weights, 'fs', ring(4, 1))  3.12 us
  transfers between devices with their start and end apart: 8, of which 2 were waited for; matrix products, arithmetic and copies ran while one was open for 5% of the time, Pallas kernels for 18%

profile of v1, /device:TPU:1, one launch (start us, length us, event | category | flops | bytes accessed | tf_op | source)
XLA Modules:
  0.0 85.1 jit_solution(8180699094994377029)
XLA Ops:
  0.6 0.0 copy-start.11
  0.7 0.7 copy-done.11
  1.3 0.0 copy-start.10
  1.3 0.8 copy.19
  2.1 0.0 copy-done.10
  2.1 0.1 copy.20
  2.2 0.0 copy-start.12
  2.2 0.0 copy-start.13
  2.3 0.0 copy-start.14
  2.3 0.0 copy-start.15
  2.3 0.7 pad.4.key_ref
  3.0 0.0 copy-done.12
  3.0 0.0 copy-done.13
  3.0 0.0 copy-done.14
  3.0 0.0 copy-done.15
  3.0 1.3 %fusion.2 = (f32[256,128]{1,0:T(8,128)}, f32[256,128]{1,0:T(8,128)}) fusion(f32[128]{0:T(128)S(1)} %copy-done.14, f32[128]{0:T(128)S(1)} %copy-done.15, f32[256]{0:T(256)S(1)} %add_convert_fusion.1, f32[128]{0:T(128)S(1)} %copy-done.13, pred[128]{0:T(512)(128)(4,1)S(1)} %copy-done.12), kind=kLoop, calls=%fused_computation.5 | loop fusion | flops 98304 | bytes 264832 | tf_op jit(solution)/shard_map/mul | solution.py:309
  4.3 3.9 %send.1 = bf16[8,432,128]{2,1,0:T(8,128)(2,1)} custom-call(s32[1]{0:T(128)} %bitcast.tp_ref, bf16[256,512]{1,0:T(8,128)(2,1)} %bitcast.20, bf16[256,512]{1,0:T(8,128)(2,1)} %bitcast.22, f32[2,512]{1,0:T(2,128)} %floor_ref.3, f32[256,4]{1,0:T(8,128)} %bitcast.18, bf16[256,256]{1,0:T(8,128)(2,1)} %bitcast.25, f32[1,256]{1,0:T(1,128)} %bitcast.28, ...), custom_call_target="tpu_custom_call" | custom-call | flops 536870912 | bytes 1048576 | tf_op jit(solution)/shard_map/send/pallas_call | solution.py:257
  8.2 0.0 copy-start.5
  8.2 7.8 %all-to-all-start = ((bf16[8,432,128]{2,1,0:T(8,128)(2,1)}), bf16[8,432,128]{2,1,0:T(8,128)(2,1)S(1)}, u32[]{:S(2)}, u32[]{:S(2)}) async-start(bf16[8,432,128]{2,1,0:T(8,128)(2,1)} %send.1), calls=%async_computation | async-start | bytes 1769472 | tf_op jit(solution)/shard_map/all_to_all | solution.py:279
  16.0 0.0 copy-done.5
  16.0 0.0 copy-start.8
  16.1 0.9 %copy-done.8 = bf16[256,512]{1,0:T(8,128)(2,1)S(1)} copy-done((bf16[256,512]{1,0:T(8,128)(2,1)S(1)}, bf16[256,512]{1,0:T(8,128)(2,1)}, u32[]{:S(2)}) %copy-start.8) | copy-done | bytes 262168
  17.0 0.0 copy-start.1
  17.0 3.1 %collective-permute-start.1 = (bf16[768,512]{1,0:T(8,128)(2,1)S(1)}, bf16[768,512]{1,0:T(8,128)(2,1)S(1)}, u32[]{:S(2)}, u32[]{:S(2)}) collective-permute-start(bf16[768,512]{1,0:T(8,128)(2,1)S(1)} %constant_dynamic-update-slice_fusion.own_ref), channel_id=1, source_target_pairs={{0,2},{2,4},{4,6},{6,0},{1,3},{3,5},{5,7},{7,1},{8,10},{10,12},{12... | collective-permute-start | bytes 2359304 | tf_op jit(solution)/shard_map/ppermute | solution.py:325
  20.1 3.4 %collective-permute-start.2 = (bf16[768,512]{1,0:T(8,128)(2,1)S(1)}, bf16[768,512]{1,0:T(8,128)(2,1)S(1)}, u32[]{:S(2)}, u32[]{:S(2)}) collective-permute-start(bf16[768,512]{1,0:T(8,128)(2,1)S(1)} %constant_dynamic-update-slice_fusion.own_ref), channel_id=1, source_target_pairs={{0,6},{2,0},{4,2},{6,4},{1,7},{3,1},{5,3},{7,5},{8,14},{10,8},{12,... | collective-permute-start | bytes 2359304 | tf_op jit(solution)/shard_map/ppermute | solution.py:326
  23.5 16.1 %all-to-all-done.got_ref.mine_ref = bf16[8,432,128]{2,1,0:T(8,128)(2,1)S(1)} async-done(((bf16[8,432,128]{2,1,0:T(8,128)(2,1)}), bf16[8,432,128]{2,1,0:T(8,128)(2,1)S(1)}, u32[]{:S(2)}, u32[]{:S(2)}) %all-to-all-start) | async-done | bytes 884768 | tf_op jit(solution)/shard_map/all_to_all | solution.py:279
  39.6 0.0 copy-start
  39.6 0.9 %slice.12 = bf16[8,288,128]{2,1,0:T(8,128)(2,1)} slice(bf16[8,432,128]{2,1,0:T(8,128)(2,1)S(1)} %all-to-all-done.got_ref.mine_ref), slice={[0:8], [144:432], [0:128]} | slice | bytes 1179648 | tf_op jit(solution)/shard_map/slice | solution.py:345
  40.5 4.5 %collective-permute-start = (bf16[8,288,128]{2,1,0:T(8,128)(2,1)}, bf16[8,288,128]{2,1,0:T(8,128)(2,1)}, u32[]{:S(2)}, u32[]{:S(2)}) collective-permute-start(bf16[8,288,128]{2,1,0:T(8,128)(2,1)} %slice.12), channel_id=1, source_target_pairs={{0,1},{1,0},{2,3},{3,2},{4,5},{5,4},{6,7},{7,6},{8,9},{9,8},{10,11... | collective-permute-start | bytes 1769480 | tf_op jit(solution)/shard_map/ppermute | solution.py:345
  45.0 0.0 copy-done
  45.0 1.9 %scan.1 = bf16[8,128,128]{2,1,0:T(8,128)(2,1)} custom-call(s32[1]{0:T(128)} %bitcast.9.dir_ref, bf16[8,432,128]{2,1,0:T(8,128)(2,1)} %copy-done), custom_call_target="tpu_custom_call" | custom-call | flops 67108864 | bytes 1048576 | tf_op jit(solution)/shard_map/scan/pallas_call | solution.py:257
  47.0 3.4 %all-to-all-start.1 = ((bf16[8,128,128]{2,1,0:T(8,128)(2,1)}), bf16[8,128,128]{2,1,0:T(8,128)(2,1)S(1)}, u32[]{:S(2)}, u32[]{:S(2)}) async-start(bf16[8,128,128]{2,1,0:T(8,128)(2,1)} %scan.1), calls=%async_computation.1 | async-start | bytes 524288 | tf_op jit(solution)/shard_map/all_to_all | solution.py:279
  50.4 0.0 collective-permute-done.1.left_ref
  50.4 0.0 copy-start.2
  50.4 0.9 %slice.13 = bf16[384,512]{1,0:T(8,128)(2,1)} slice(bf16[768,512]{1,0:T(8,128)(2,1)S(1)} %collective-permute-done.1.left_ref), slice={[0:384], [0:512]} | slice | bytes 786432 | tf_op jit(solution)/shard_map/slice | solution.py:327
  51.3 3.1 %collective-permute-start.3 = (bf16[384,512]{1,0:T(8,128)(2,1)}, bf16[384,512]{1,0:T(8,128)(2,1)S(1)}, u32[]{:S(2)}, u32[]{:S(2)}) collective-permute-start(bf16[384,512]{1,0:T(8,128)(2,1)} %slice.13), channel_id=1, source_target_pairs={{0,2},{2,4},{4,6},{6,0},{1,3},{3,5},{5,7},{7,1},{8,10},{10,12},{12... | collective-permute-start | bytes 1179656 | tf_op jit(solution)/shard_map/ppermute | solution.py:327
  54.4 0.0 collective-permute-done.2.right_ref
  54.4 0.0 copy-start.3
  54.4 0.8 slice.14
  55.2 0.0 copy-done.2
  55.2 3.5 %collective-permute-start.4 = (bf16[384,512]{1,0:T(8,128)(2,1)}, bf16[384,512]{1,0:T(8,128)(2,1)S(1)}, u32[]{:S(2)}, u32[]{:S(2)}) collective-permute-start(bf16[384,512]{1,0:T(8,128)(2,1)} %slice.14), channel_id=1, source_target_pairs={{0,6},{2,0},{4,2},{6,4},{1,7},{3,1},{5,3},{7,5},{8,14},{10,8},{12,... | collective-permute-start | bytes 1179656 | tf_op jit(solution)/shard_map/ppermute | solution.py:328
  58.8 0.6 stack.23.idx_ref
  59.5 7.1 %local.1 = (f32[256,512]{1,0:T(8,128)}, bf16[2,256,512]{2,1,0:T(8,128)(2,1)}) custom-call(bf16[256,512]{1,0:T(8,128)(2,1)} %bitcast.29, bf16[256,512]{1,0:T(8,128)(2,1)} %bitcast.21, bf16[256,512]{1,0:T(8,128)(2,1)} %bitcast.23, f32[2,512]{1,0:T(2,128)} %floor_ref.3, f32[256,4]{1,0:T(8,128)} %bitcast.19), custom_call_target="tpu_custom_call" | custom-call | flops 1073741824 | bytes 1048576 | tf_op jit(solution)/shard_map/local/pallas_call | solution.py:257
  66.5 0.0 copy-done.1
  66.5 0.0 copy-done.3
  66.5 0.0 collective-permute-done.other_ref
  66.5 6.5 %attend.1 = (bf16[256,256]{1,0:T(8,128)(2,1)}, f32[256,4]{1,0:T(8,128)}) custom-call(s32[1]{0:T(128)} %bitcast.tp_ref, bf16[256,384]{1,0:T(8,128)(2,1)} %bitcast.30, bf16[8,432,128]{2,1,0:T(8,128)(2,1)} %copy-done, bf16[8,288,128]{2,1,0:T(8,128)(2,1)} %collective-permute-done.other_ref, bf16[256,1024]{1,0:T(8,128)(2,1)} %up_ref.1, ...), custom_call_target="tpu_custom_call" | custom-call | flops 2147483648 | bytes 1048576 | tf_op jit(solution)/shard_map/attend/pallas_call | solution.py:257
  73.1 0.0 collective-permute-done.3.far_a_ref
  73.1 0.0 copy-start.6
  73.1 0.0 collective-permute-done.4.far_b_ref
  73.1 0.0 copy-start.7
  73.1 0.0 all-to-all-done.1.state_ref
  73.1 0.0 copy-start.4
  73.1 0.8 copy-done.6
  73.9 0.1 copy-done.7
  74.0 0.1 copy-done.4
  74.1 0.0 copy-start.9
  74.1 4.8 %finish.1 = (bf16[128,2048]{1,0:T(8,128)(2,1)}, bf16[128,2048]{1,0:T(8,128)(2,1)}) custom-call(s32[5]{0:T(128)} %stack.23.idx_ref, f32[256,512]{1,0:T(8,128)} %get-tuple-element.8.local_ref, bf16[2,256,512]{2,1,0:T(8,128)(2,1)} %get-tuple-element.9.damped_ref, bf16[8,128,128]{2,1,0:T(8,128)(2,1)} %copy-done.4, f32[1,512]{1,0:T(1,128)} %bitcast.27, ...), custom_call_target="tpu_custom_call" | custom-call | flops 1073741824 | bytes 1048576 | tf_op jit(solution)/shard_map/finish/pallas_call | solution.py:257
  78.9 2.5 %collective-permute-start.5 = (bf16[128,2048]{1,0:T(8,128)(2,1)}, bf16[128,2048]{1,0:T(8,128)(2,1)S(1)}, u32[]{:S(2)}, u32[]{:S(2)}) collective-permute-start(bf16[128,2048]{1,0:T(8,128)(2,1)} %get-tuple-element.12), channel_id=1, source_target_pairs={{0,1},{1,0},{2,3},{3,2},{4,5},{5,4},{6,7},{7,6},{8,9},{9,8},{10,11... | collective-permute-start | bytes 1572872 | tf_op jit(solution)/shard_map/ppermute | solution.py:363
  81.4 0.0 copy-done.9
  81.4 0.7 copy.21
  82.1 1.0 %collective-permute-done.5 = bf16[128,2048]{1,0:T(8,128)(2,1)S(1)} collective-permute-done((bf16[128,2048]{1,0:T(8,128)(2,1)}, bf16[128,2048]{1,0:T(8,128)(2,1)S(1)}, u32[]{:S(2)}, u32[]{:S(2)}) %collective-permute-start.5) | collective-permute-done | bytes 524320 | tf_op jit(solution)/shard_map/ppermute | solution.py:363
  83.1 2.0 %fusion = bf16[1,128,2048]{2,1,0:T(8,128)(2,1)} fusion(bf16[128,2048]{1,0:T(8,128)(2,1)S(1)} %collective-permute-done.5, bf16[128,2048]{1,0:T(8,128)(2,1)} %get-tuple-element.11), kind=kLoop, calls=%fused_computation.1 | loop fusion | flops 1048576 | bytes 1572864 | tf_op jit(solution)/shard_map/broadcast_in_dim | solution.py:365
  (3 shorter events, 0.1 us)
Async XLA Ops:
  0.6 0.7 copy-start.11
  1.3 0.8 copy-start.10
  2.2 0.8 copy-start.12
  2.2 0.8 copy-start.13
  2.3 0.8 copy-start.14
  2.3 0.7 copy-start.15
  8.2 7.8 %copy-start.5 = (bf16[512,512]{1,0:T(8,128)(2,1)S(1)}, bf16[512,512]{1,0:T(8,128)(2,1)}, u32[]{:S(2)}) copy-start(bf16[512,512]{1,0:T(8,128)(2,1)} %param.28) | copy-start | bytes 1572868
  8.2 31.3 %all-to-all-start = ((bf16[8,432,128]{2,1,0:T(8,128)(2,1)}), bf16[8,432,128]{2,1,0:T(8,128)(2,1)S(1)}, u32[]{:S(2)}, u32[]{:S(2)}) async-start(bf16[8,432,128]{2,1,0:T(8,128)(2,1)} %send.1), calls=%async_computation | async-start | bytes 1769472 | tf_op jit(solution)/shard_map/all_to_all | solution.py:279
  16.0 1.0 %copy-start.8 = (bf16[256,512]{1,0:T(8,128)(2,1)S(1)}, bf16[256,512]{1,0:T(8,128)(2,1)}, u32[]{:S(2)}) copy-start(bf16[256,512]{1,0:T(8,128)(2,1)} %param.29) | copy-start | bytes 786436
  17.0 49.5 %copy-start.1 = (bf16[768,512]{1,0:T(8,128)(2,1)}, bf16[768,512]{1,0:T(8,128)(2,1)S(1)}, u32[]{:S(2)}) copy-start(bf16[768,512]{1,0:T(8,128)(2,1)S(1)} %constant_dynamic-update-slice_fusion.own_ref) | copy-start | bytes 2359300
  17.0 33.4 %collective-permute-start.1 = (bf16[768,512]{1,0:T(8,128)(2,1)S(1)}, bf16[768,512]{1,0:T(8,128)(2,1)S(1)}, u32[]{:S(2)}, u32[]{:S(2)}) collective-permute-start(bf16[768,512]{1,0:T(8,128)(2,1)S(1)} %constant_dynamic-update-slice_fusion.own_ref), channel_id=1, source_target_pairs={{0,2},{2,4},{4,6},{6,0},{1,3},{3,5},{5,7},{7,1},{8,10},{10,12},{12... | collective-permute-start | bytes 2359304 | tf_op jit(solution)/shard_map/ppermute | solution.py:325
  20.1 34.3 %collective-permute-start.2 = (bf16[768,512]{1,0:T(8,128)(2,1)S(1)}, bf16[768,512]{1,0:T(8,128)(2,1)S(1)}, u32[]{:S(2)}, u32[]{:S(2)}) collective-permute-start(bf16[768,512]{1,0:T(8,128)(2,1)S(1)} %constant_dynamic-update-slice_fusion.own_ref), channel_id=1, source_target_pairs={{0,6},{2,0},{4,2},{6,4},{1,7},{3,1},{5,3},{7,5},{8,14},{10,8},{12,... | collective-permute-start | bytes 2359304 | tf_op jit(solution)/shard_map/ppermute | solution.py:326
  39.6 5.5 %copy-start = (bf16[8,432,128]{2,1,0:T(8,128)(2,1)}, bf16[8,432,128]{2,1,0:T(8,128)(2,1)S(1)}, u32[]{:S(2)}) copy-start(bf16[8,432,128]{2,1,0:T(8,128)(2,1)S(1)} %all-to-all-done.got_ref.mine_ref) | copy-start | bytes 2654212
  40.5 26.0 %collective-permute-start = (bf16[8,288,128]{2,1,0:T(8,128)(2,1)}, bf16[8,288,128]{2,1,0:T(8,128)(2,1)}, u32[]{:S(2)}, u32[]{:S(2)}) collective-permute-start(bf16[8,288,128]{2,1,0:T(8,128)(2,1)} %slice.12), channel_id=1, source_target_pairs={{0,1},{1,0},{2,3},{3,2},{4,5},{5,4},{6,7},{7,6},{8,9},{9,8},{10,11... | collective-permute-start | bytes 1769480 | tf_op jit(solution)/shard_map/ppermute | solution.py:345
  47.0 26.1 %all-to-all-start.1 = ((bf16[8,128,128]{2,1,0:T(8,128)(2,1)}), bf16[8,128,128]{2,1,0:T(8,128)(2,1)S(1)}, u32[]{:S(2)}, u32[]{:S(2)}) async-start(bf16[8,128,128]{2,1,0:T(8,128)(2,1)} %scan.1), calls=%async_computation.1 | async-start | bytes 524288 | tf_op jit(solution)/shard_map/all_to_all | solution.py:279
  50.4 4.8 %copy-start.2 = (bf16[768,512]{1,0:T(8,128)(2,1)}, bf16[768,512]{1,0:T(8,128)(2,1)S(1)}, u32[]{:S(2)}) copy-start(bf16[768,512]{1,0:T(8,128)(2,1)S(1)} %collective-permute-done.1.left_ref) | copy-start | bytes 2359300
  51.3 21.8 %collective-permute-start.3 = (bf16[384,512]{1,0:T(8,128)(2,1)}, bf16[384,512]{1,0:T(8,128)(2,1)S(1)}, u32[]{:S(2)}, u32[]{:S(2)}) collective-permute-start(bf16[384,512]{1,0:T(8,128)(2,1)} %slice.13), channel_id=1, source_target_pairs={{0,2},{2,4},{4,6},{6,0},{1,3},{3,5},{5,7},{7,1},{8,10},{10,12},{12... | collective-permute-start | bytes 1179656 | tf_op jit(solution)/shard_map/ppermute | solution.py:327
  54.4 12.1 %copy-start.3 = (bf16[768,512]{1,0:T(8,128)(2,1)}, bf16[768,512]{1,0:T(8,128)(2,1)S(1)}, u32[]{:S(2)}) copy-start(bf16[768,512]{1,0:T(8,128)(2,1)S(1)} %collective-permute-done.2.right_ref) | copy-start | bytes 2359300
  55.2 17.8 %collective-permute-start.4 = (bf16[384,512]{1,0:T(8,128)(2,1)}, bf16[384,512]{1,0:T(8,128)(2,1)S(1)}, u32[]{:S(2)}, u32[]{:S(2)}) collective-permute-start(bf16[384,512]{1,0:T(8,128)(2,1)} %slice.14), channel_id=1, source_target_pairs={{0,6},{2,0},{4,2},{6,4},{1,7},{3,1},{5,3},{7,5},{8,14},{10,8},{12,... | collective-permute-start | bytes 1179656 | tf_op jit(solution)/shard_map/ppermute | solution.py:328
  73.1 0.8 copy-start.6
  73.1 0.9 %copy-start.7 = (bf16[384,512]{1,0:T(8,128)(2,1)}, bf16[384,512]{1,0:T(8,128)(2,1)S(1)}, u32[]{:S(2)}) copy-start(bf16[384,512]{1,0:T(8,128)(2,1)S(1)} %collective-permute-done.4.far_b_ref) | copy-start | bytes 1179652
  73.1 1.0 %copy-start.4 = (bf16[8,128,128]{2,1,0:T(8,128)(2,1)}, bf16[8,128,128]{2,1,0:T(8,128)(2,1)S(1)}, u32[]{:S(2)}) copy-start(bf16[8,128,128]{2,1,0:T(8,128)(2,1)S(1)} %all-to-all-done.1.state_ref) | copy-start | bytes 786436
  74.1 7.3 %copy-start.9 = (f32[256,4]{1,0:T(8,128)S(1)}, f32[256,4]{1,0:T(8,128)}, u32[]{:S(2)}) copy-start(f32[256,4]{1,0:T(8,128)} %get-tuple-element.13) | copy-start | bytes 12292
  78.9 4.2 %collective-permute-start.5 = (bf16[128,2048]{1,0:T(8,128)(2,1)}, bf16[128,2048]{1,0:T(8,128)(2,1)S(1)}, u32[]{:S(2)}, u32[]{:S(2)}) collective-permute-start(bf16[128,2048]{1,0:T(8,128)(2,1)} %get-tuple-element.12), channel_id=1, source_target_pairs={{0,1},{1,0},{2,3},{3,2},{4,5},{5,4},{6,7},{7,6},{8,9},{9,8},{10,11... | collective-permute-start | bytes 1572872 | tf_op jit(solution)/shard_map/ppermute | solution.py:363

commit v2 on v1

v2 whole, which is shorter than its diff:
```python
import numpy as np

import jax
import jax.numpy as jnp
from jax import lax
from jax.experimental import pallas as pl
from jax.experimental.pallas import tpu as pltpu
from jax.sharding import Mesh
from jax.sharding import PartitionSpec as P


DK = 128
HEADS = 4
NOPE = 64
ROPE = 32
RANK = 256
BLOCK = 64
TOK = 256
HALF = 128
SEQ_DEV = 8
STATE_ROWS = 144
KV_ROWS = 288
CHUNK_ROWS = STATE_ROWS + KV_ROWS
SP = ("sp_0", "sp_1")
SP_TP = ("sp_0", "sp_1", "tp")
EPS = 1e-06
ROPE_BASE = 10000.0
SCALE = (NOPE + ROPE) ** (-0.5)
LOG2E = 1.4426950408889634

f32 = jnp.float32
bf16 = jnp.bfloat16
NT = (((1,), (1,)), ((), ()))
TN = (((0,), (0,)), ((), ()))


def dot(a, b, dims=(((1,), (0,)), ((), ()))):
    return lax.dot_general(a, b, dims, preferred_element_type=f32)


def iota2(shape, axis):
    return lax.broadcasted_iota(jnp.int32, shape, axis)


def exact_sum(selector, values):
    high = values.astype(bf16)
    low = (values - high.astype(f32)).astype(bf16)
    return dot(selector, high) + dot(selector, low)


def start_all(sems, pairs):
    copies = [pltpu.make_async_copy(src, dst, sems.at[i]) for i, (src, dst) in enumerate(pairs)]
    for copy in copies:
        copy.start()
    return copies


def shut(logit):
    return 0.5 - 0.5 * jnp.tanh(0.5 * logit)


def gate(closed, floor, extra):
    keyed = (1.0 - floor) * closed
    return keyed, jnp.log(1.0 - keyed) + extra


def head_extra(extra_ref, first, count):
    return jnp.concatenate(
        [
            jnp.transpose(jnp.broadcast_to(extra_ref[h : h + 1, :], (DK, TOK)))
            for h in range(first, first + count)
        ],
        axis=1,
    )


def rotated(x, cos_table, sin_table):
    lane = iota2(x.shape, 1)
    partner = jnp.where(lane < NOPE + ROPE // 2, pltpu.roll(x, 128 - 16, 1), pltpu.roll(x, 16, 1))
    return x * cos_table + partner * sin_table


def send_kernel(
    logit_hbm, value_hbm, floor_hbm, extra_hbm, lat_hbm, gain_hbm, key_hbm, cos_hbm, sin_hbm,
    upper_hbm, lower_hbm,
    out_hbm, weight_hbm,
    logit_ref, value_ref, floor_ref, extra_ref, lat_ref, gain_ref, key_ref, cos_ref, sin_ref,
    state_ref, kv_ref, weight_ref, in_sems, kv_sems, state_sems, weight_sem,
):
    tp, place = lax.axis_index("tp"), lax.axis_index("sp_1")
    mine = pl.ds(pl.multiple_of(tp * HALF, HALF), HALF)
    spot = pl.ds(pl.multiple_of(place * TOK + tp * HALF, HALF), HALF)
    loads = start_all(
        in_sems,
        [
            (lat_hbm.at[mine, :], lat_ref),
            (gain_hbm, gain_ref),
            (key_hbm, key_ref),
            (cos_hbm.at[:, spot], cos_ref),
            (sin_hbm.at[:, spot], sin_ref),
            (logit_hbm, logit_ref),
            (extra_hbm, extra_ref),
            (floor_hbm, floor_ref),
            (value_hbm, value_ref),
            (upper_hbm, weight_ref.at[0:512, :]),
            (lower_hbm, weight_ref.at[512:768, :]),
        ],
    )
    for load in loads[:5]:
        load.wait()
    wide = lat_ref[...].astype(f32)
    mean = jnp.sum(wide * wide, axis=1, keepdims=True) * (1.0 / RANK)
    normed = (wide * lax.rsqrt(mean + EPS) * gain_ref[...]).astype(bf16)
    key = key_ref[:, mine].astype(f32)
    cos, sin = cos_ref[...], sin_ref[...]
    turned = jnp.concatenate(
        [key[:16] * cos - key[16:] * sin, key[:16] * sin + key[16:] * cos], axis=0
    ).astype(bf16)
    kv_ref[0:128, :] = normed[:, :128]
    kv_ref[128:256, :] = normed[:, 128:]
    kv_ref[256:KV_ROWS, :] = turned
    stores = start_all(
        kv_sems,
        [(kv_ref, out_hbm.at[q, STATE_ROWS:CHUNK_ROWS, :]) for q in range(SEQ_DEV)],
    )
    for load in loads[5:9]:
        load.wait()
    rows = iota2((TOK, TOK), 0)
    cols = iota2((TOK, TOK), 1)
    after = (cols > rows).astype(f32).astype(bf16)
    before = (cols < rows).astype(f32).astype(bf16)
    for pair in range(HEADS // 2):
        if pair == 1:
            for load in loads[9:]:
                load.wait()
            weight_store = pltpu.make_async_copy(weight_ref, weight_hbm, weight_sem)
            weight_store.start()
            stores.append(weight_store)
        lanes = slice(pair * 2 * DK, (pair + 1) * 2 * DK)
        closed = shut(logit_ref[:, lanes].astype(f32))
        extra = head_extra(extra_ref, 2 * pair, 2)
        for d in range(2):
            keyed, decay = gate(closed, floor_ref[d : d + 1, lanes], extra)
            left = exact_sum(after if d == 0 else before, decay)
            edge = 0 if d == 0 else TOK - 1
            total = jnp.exp(left[edge : edge + 1] + decay[edge : edge + 1])
            weighted = (keyed * jnp.exp(left)).astype(bf16)
            for s in range(2):
                h = 2 * pair + s
                at = d * HEADS + h
                state = dot(
                    value_ref[:, h * DK : (h + 1) * DK], weighted[:, s * DK : (s + 1) * DK], TN
                )
                state_ref[at, 0:DK, :] = state.astype(bf16)
                state_ref[at, DK:STATE_ROWS, :] = jnp.broadcast_to(
                    total[:, s * DK : (s + 1) * DK], (STATE_ROWS - DK, DK)
                ).astype(bf16)
                store = pltpu.make_async_copy(
                    state_ref.at[at], out_hbm.at[at, 0:STATE_ROWS, :], state_sems.at[at]
                )
                store.start()
                stores.append(store)
    for store in stores:
        store.wait()


def local_kernel(
    query_ref, logit_ref, value_ref, floor_ref, extra_ref, out_hbm, damped_hbm, out_ref, damped_ref, sems
):
    stores = []
    rows = iota2((TOK, TOK), 0)
    cols = iota2((TOK, TOK), 1)
    same = (rows // BLOCK) == (cols // BLOCK)
    lower = same & (cols <= rows)
    upper = same & (cols >= rows)
    blocks = TOK // BLOCK
    for h in range(HEADS):
        lanes = slice(h * DK, (h + 1) * DK)
        closed = shut(logit_ref[:, lanes].astype(f32))
        extra = head_extra(extra_ref, h, 1)
        query = query_ref[:, lanes].astype(f32)
        value = value_ref[:, lanes]
        outs = [None] * blocks
        inner_sum = jnp.zeros((TOK, DK), f32)
        for d in range(2):
            seen = lower if d == 0 else upper
            keyed, decay = gate(closed, floor_ref[d : d + 1, lanes], extra)
            within = exact_sum(seen.astype(f32).astype(bf16), decay)
            damped = query * jnp.exp(within)
            grown = (keyed * jnp.exp(-within)).astype(bf16)
            damped16 = damped.astype(bf16)
            scores = jnp.where(seen, dot(damped16, grown, NT), 0.0).astype(bf16)
            inner_sum = inner_sum + dot(scores, value)
            state = None
            offset = jnp.zeros((1, DK), f32)
            for b in range(blocks) if d == 0 else reversed(range(blocks)):
                at = slice(b * BLOCK, (b + 1) * BLOCK)
                edge = (b + 1) * BLOCK - 1 if d == 0 else b * BLOCK
                total = within[edge : edge + 1]
                damped_ref[d, at, lanes] = (damped[at] * jnp.exp(offset)).astype(bf16)
                if state is not None:
                    cross = dot(damped16[at], state.astype(bf16), NT)
                    outs[b] = cross if outs[b] is None else outs[b] + cross
                offset = offset + total
                if b == (blocks - 1 if d == 0 else 0):
                    continue
                weighted = (keyed[at] * jnp.exp(total - within[at])).astype(bf16)
                added = dot(value[at], weighted, TN)
                state = added if state is None else state * jnp.exp(total) + added
        for b in range(blocks):
            at = slice(b * BLOCK, (b + 1) * BLOCK)
            out_ref[at, lanes] = inner_sum[at] if outs[b] is None else inner_sum[at] + outs[b]
        stores.append(pltpu.make_async_copy(out_ref.at[:, lanes], out_hbm.at[:, lanes], sems.at[h, 0]))
        stores.append(
            pltpu.make_async_copy(damped_ref.at[:, :, lanes], damped_hbm.at[:, :, lanes], sems.at[h, 1])
        )
        for store in stores[-2:]:
            store.start()
    for store in stores:
        store.wait()


def scan_kernel(got_ref, out_ref):
    d = lax.axis_index("sp_1") // HEADS
    carried = jnp.zeros((DK, DK), f32)
    for k in range(SEQ_DEV):
        j = jnp.where(d == 0, k, SEQ_DEV - 1 - k)
        out_ref[j] = carried.astype(bf16)
        if k < SEQ_DEV - 1:
            decay = got_ref[j, DK:STATE_ROWS, :][0:1].astype(f32)
            carried = carried * decay + got_ref[j, 0:DK, :].astype(f32)


def unpack_rope(rope_ref, ref, base):
    for j in range(SEQ_DEV):
        turned = ref[j, base + 256 : base + 288, :].astype(f32)
        rope_ref[j * 128 : j * 128 + 128, :] = jnp.transpose(
            jnp.concatenate([jnp.zeros((NOPE, 128), f32), turned, jnp.zeros((32, 128), f32)], axis=0)
        ).astype(bf16)


def expand(ex_ref, ref, base, up_ref):
    up = up_ref[:, pl.ds(pl.multiple_of(lax.axis_index("tp") * HEADS * 128, HEADS * 128), HEADS * 128)]
    for j in range(SEQ_DEV):
        lat = jnp.concatenate(
            [ref[j, base : base + 128, :], ref[j, base + 128 : base + 256, :]], axis=1
        )
        ex_ref[j * 128 : j * 128 + 128, :] = dot(lat, up).astype(bf16)


def expand_kernel(got_ref, up_ref, ex_ref, rope_ref):
    unpack_rope(rope_ref, got_ref, STATE_ROWS)
    expand(ex_ref, got_ref, STATE_ROWS, up_ref)


def attend_kernel(
    query_ref, other_ref, ex_mine_ref, rope_mine_ref, up_ref, cos_ref, sin_ref, local_hbm, damped_hbm,
    gain_hbm,
    out_ref, lw_ref, local_ref, damped_ref, gain_ref,
    ex_ref, rope_ref, sems,
):
    loads = start_all(
        sems, [(local_hbm, local_ref), (damped_hbm, damped_ref), (gain_hbm, gain_ref)]
    )
    unpack_rope(rope_ref, other_ref, 0)
    expand(ex_ref, other_ref, 0, up_ref)
    spot = pl.ds(pl.multiple_of(lax.axis_index("sp_1") * TOK, TOK), TOK)
    cos, sin = cos_ref[:, spot], sin_ref[:, spot]
    nothing = jnp.zeros((NOPE, TOK), f32)
    cos_table = jnp.transpose(jnp.concatenate([nothing + 1.0, cos, cos, nothing[:32]], axis=0))
    sin_table = jnp.transpose(jnp.concatenate([nothing, -sin, sin, nothing[:32]], axis=0))
    log_weights = []
    lane = iota2((TOK, 128), 1)
    q_blocks = [query_ref[:, 128 * i : 128 * i + 128].astype(f32) for i in range(3)]
    key_lane = iota2((SEQ_DEV * HALF, 128), 1)
    for h in range(HEADS):
        lanes = slice(h * 128, (h + 1) * 128)
        if h == 0:
            q = q_blocks[0]
        elif h == 1:
            q = jnp.where(lane < 32, pltpu.roll(q_blocks[0], 32, 1), pltpu.roll(q_blocks[1], 32, 1))
        elif h == 2:
            q = jnp.where(lane < 64, pltpu.roll(q_blocks[1], 64, 1), pltpu.roll(q_blocks[2], 64, 1))
        else:
            q = pltpu.roll(q_blocks[2], 96, 1)
        q = rotated(q, cos_table, sin_table).astype(bf16)
        parts = []
        for ex_part, rope_part in ((ex_mine_ref, rope_mine_ref), (ex_ref, rope_ref)):
            ex = ex_part[:, lanes]
            parts.append((ex, dot(q, jnp.where(key_lane < NOPE, ex, rope_part[...]), NT)))
        peak = jnp.maximum(
            jnp.max(parts[0][1], axis=1, keepdims=True), jnp.max(parts[1][1], axis=1, keepdims=True)
        )
        total, mixed = 0.0, 0.0
        for ex, scores in parts:
            weights = jnp.exp2((scores - peak) * (SCALE * LOG2E))
            total = total + jnp.sum(weights, axis=1, keepdims=True)
            mixed = mixed + dot(weights.astype(bf16), ex)
        mixed = mixed / total
        log_weights.append(jnp.broadcast_to(peak * SCALE + jnp.log(total), (TOK, 32)))
        if h % 2 == 0:
            kept = pltpu.roll(mixed, 64, 1)
        else:
            out_ref[:, (h // 2) * 128 : (h // 2) * 128 + 128] = jnp.where(
                lane < 64, kept, mixed
            ).astype(bf16)
    turned = jnp.transpose(jnp.concatenate(log_weights, axis=1))
    for h in range(HEADS):
        lw_ref[h : h + 1, :] = turned[32 * h : 32 * h + 1]
    for load in loads:
        load.wait()


def finish_kernel(
    local_ref, damped_ref, state_ref, gain_ref, att_ref, own_hbm, left_hbm, right_hbm, far_hbm,
    send_ref, keep_ref,
    weight_ref, act_ref, sems,
):
    tp, column = lax.axis_index("tp"), lax.axis_index("fs")
    loads = start_all(
        sems,
        [(ref, weight_ref.at[i]) for i, ref in enumerate((own_hbm, left_hbm, right_hbm, far_hbm))],
    )
    for part in range(2):
        start = jnp.where(tp == part, HALF, 0)
        at = pl.ds(pl.multiple_of(start, HALF), HALF)
        to = slice(part * HALF, (part + 1) * HALF)
        for h in range(HEADS):
            lanes = slice(h * DK, (h + 1) * DK)
            o = (
                local_ref[at, lanes]
                + dot(damped_ref[0, at, lanes], state_ref[h], NT)
                + dot(damped_ref[1, at, lanes], state_ref[HEADS + h], NT)
            )
            mean = jnp.sum(o * o, axis=1, keepdims=True) * (1.0 / DK)
            act_ref[to, lanes] = (o * lax.rsqrt(mean + EPS) * gain_ref[:, lanes]).astype(bf16)
        act_ref[to, HEADS * DK :] = att_ref[at, :]
    act = act_ref[...]
    for i in range(4):
        loads[i].wait()
        got = dot(act, weight_ref[i]).astype(bf16)
        lanes = pl.ds(pl.multiple_of(((column + (0, 3, 1, 2)[i]) % 4) * 512, 512), 512)
        send_ref[:, lanes] = got[:HALF]
        keep_ref[:, lanes] = got[HALF:]


SPACES = {"v": pltpu.VMEM, "h": pltpu.HBM}


def call(kernel, ins, outs, *args, scratch=(), flops=0, mib=16):
    args = [
        pltpu.with_memory_space_constraint(a, pltpu.HBM) if c == "h" else a for c, a in zip(ins, args)
    ]
    many = isinstance(outs, tuple)
    spaces = [
        pltpu.HBM if isinstance(o, HbmOut) else pltpu.VMEM for o in (outs if many else (outs,))
    ]
    shapes = tuple(
        pltpu.HBM(o.dims, o.dtype) if isinstance(o, HbmOut) else o for o in (outs if many else (outs,))
    )
    specs = tuple(pl.BlockSpec(memory_space=space) for space in spaces)
    return pl.pallas_call(
        kernel,
        out_shape=shapes if many else shapes[0],
        in_specs=[pl.BlockSpec(memory_space=SPACES[c]) for c in ins],
        out_specs=specs if many else specs[0],
        scratch_shapes=list(scratch),
        cost_estimate=pl.CostEstimate(flops=flops, bytes_accessed=1 << 20, transcendentals=0),
        compiler_params=pltpu.CompilerParams(vmem_limit_bytes=mib << 20),
    )(*args)


class HbmOut:
    def __init__(self, dims, dtype):
        self.dims, self.dtype = dims, dtype


def shape(dims, dtype):
    return jax.ShapeDtypeStruct(dims, dtype)


def ring(n, step):
    return [(i, (i + step) % n) for i in range(n)]


def exchange(value):
    return lax.all_to_all(value, "sp_1", split_axis=0, concat_axis=0, tiled=True)


def local(
    recurrent_query,
    forget_logits,
    recurrent_value,
    forget_floor,
    extra_log_decay,
    recurrent_norm_gain,
    attention_query,
    latent,
    rotary_key,
    latent_norm_gain,
    latent_up_weight,
    recurrent_output_weight,
    attention_output_weight,
):
    cos_table, sin_table = rotary_tables()
    logits, values = forget_logits[0], recurrent_value[0]
    extra = jnp.swapaxes(extra_log_decay[0], 0, 1)

    sent, weights = call(
        send_kernel,
        "h" * 11,
        (HbmOut((SEQ_DEV, CHUNK_ROWS, DK), bf16), HbmOut((768, 512), bf16)),
        logits, values, forget_floor, extra, latent[0], latent_norm_gain.reshape(1, RANK),
        jnp.swapaxes(rotary_key[0], 0, 1), cos_table, sin_table,
        recurrent_output_weight, attention_output_weight,
        scratch=(
            pltpu.VMEM((TOK, HEADS * DK), bf16),
            pltpu.VMEM((TOK, HEADS * DK), bf16),
            pltpu.VMEM((2, HEADS * DK), f32),
            pltpu.VMEM((HEADS, TOK), f32),
            pltpu.VMEM((HALF, RANK), bf16),
            pltpu.VMEM((1, RANK), f32),
            pltpu.VMEM((ROPE, TOK), bf16),
            pltpu.VMEM((16, HALF), f32),
            pltpu.VMEM((16, HALF), f32),
            pltpu.VMEM((2 * HEADS, STATE_ROWS, DK), bf16),
            pltpu.VMEM((KV_ROWS, DK), bf16),
            pltpu.VMEM((768, 512), bf16),
            pltpu.SemaphoreType.DMA((11,)),
            pltpu.SemaphoreType.DMA((SEQ_DEV,)),
            pltpu.SemaphoreType.DMA((2 * HEADS,)),
            pltpu.SemaphoreType.DMA,
        ),
        flops=1 << 29, mib=14,
    )
    got = exchange(sent)

    from_left = lax.ppermute(weights, "fs", ring(4, 1))
    from_right = lax.ppermute(weights, "fs", ring(4, -1))
    far = lax.ppermute(weights, "fs", ring(4, 2))

    local_out, damped = call(
        local_kernel,
        "vvvvv",
        (HbmOut((TOK, HEADS * DK), f32), HbmOut((2, TOK, HEADS * DK), bf16)),
        recurrent_query[0], logits, values, forget_floor, extra,
        scratch=(
            pltpu.VMEM((TOK, HEADS * DK), f32),
            pltpu.VMEM((2, TOK, HEADS * DK), bf16),
            pltpu.SemaphoreType.DMA((HEADS, 2)),
        ),
        flops=1 << 30, mib=14,
    )

    scanned = call(
        scan_kernel, "v", shape((SEQ_DEV, DK, DK), bf16), got,
        flops=1 << 26, mib=8,
    )
    states = exchange(scanned)

    other = lax.ppermute(got[:, STATE_ROWS:], "tp", [(0, 1), (1, 0)])
    keys = SEQ_DEV * HALF
    ex_mine, rope_mine = call(
        expand_kernel, "vv",
        (shape((keys, HEADS * 128), bf16), shape((keys, 128), bf16)),
        got, latent_up_weight,
        flops=1 << 28, mib=12,
    )
    attended, log_weight, local_out, damped, gain = call(
        attend_kernel,
        "v" * 7 + "hhh",
        (
            shape((TOK, HEADS * 64), bf16),
            shape((HEADS, TOK), f32),
            shape((TOK, HEADS * DK), f32),
            shape((2, TOK, HEADS * DK), bf16),
            shape((1, HEADS * DK), f32),
        ),
        attention_query[0], other, ex_mine, rope_mine, latent_up_weight, cos_table, sin_table,
        local_out, damped, recurrent_norm_gain.reshape(1, HEADS * DK),
        scratch=(
            pltpu.VMEM((keys, HEADS * 128), bf16),
            pltpu.VMEM((keys, 128), bf16),
            pltpu.SemaphoreType.DMA((3,)),
        ),
        flops=1 << 31, mib=24,
    )

    send, keep = call(
        finish_kernel,
        "v" * 5 + "h" * 4,
        (shape((HALF, 2048), bf16), shape((HALF, 2048), bf16)),
        local_out, damped, states, gain, attended, weights, from_left, from_right, far,
        scratch=(
            pltpu.VMEM((4, 768, 512), bf16),
            pltpu.VMEM((TOK, 768), bf16),
            pltpu.SemaphoreType.DMA((4,)),
        ),
        flops=1 << 30, mib=16,
    )
    arrived = lax.ppermute(send, "tp", [(0, 1), (1, 0)])
    mixed = (keep.astype(f32) + arrived.astype(f32)).astype(bf16)
    return mixed[None], jnp.swapaxes(log_weight, 0, 1)[None]


def rotary_tables():
    inverse = np.power(
        np.float32(ROPE_BASE), -np.arange(16, dtype=np.float32) / np.float32(16), dtype=np.float32
    )
    angle = inverse[:, None] * np.arange(SEQ_DEV * TOK, dtype=np.float32)[None, :]
    angle = angle.astype(np.float64)
    return np.cos(angle).astype(np.float32), np.sin(angle).astype(np.float32)


def solution(mesh):
    torus = Mesh(
        mesh.devices.reshape(8, 8, mesh.shape["fs"], mesh.shape["tp"]), ("sp_0", "sp_1", "fs", "tp")
    )
    in_specs = (
        P("fs", SP, "tp"),
        P("fs", SP, "tp"),
        P("fs", SP, "tp"),
        P(None, "tp"),
        P("fs", SP, "tp"),
        P("tp"),
        P("fs", SP, "tp"),
        P("fs", SP, None),
        P("fs", SP, None),
        P(),
        P(),
        P("tp", "fs"),
        P("tp", "fs"),
    )
    out_specs = (P("fs", SP_TP, None), P("fs", SP, "tp"))
    return jax.shard_map(local, mesh=torus, in_specs=in_specs, out_specs=out_specs, check_vma=False)
```

time: 85.7 us -> 89.1 us (1.040)
  blocking collectives: 0 us -> 29.8 us
  starting transfers between devices: 31.3 us -> 21.9 us
  local copies, waits for them, and re-layouts: 8.21 us -> 1.46 us
  Pallas kernels: 24.3 us -> 18.1 us
  other arithmetic: 3.24 us -> 0.92 us
  waiting for transfers between devices: 17.1 us -> 15.6 us
    all_to_all x0 -> x1, blocking collectives: none -> 29.8 us  [exchange(): lax.all_to_all(value, 'sp_1', split_axis=0, concat_axis=0, tiled=True)]
    all_to_all x2 -> x1, waiting for transfers between devices: 16.1 us -> 0.01 us  [exchange(): lax.all_to_all(value, 'sp_1', split_axis=0, concat_axis=0, tiled=True)]
    ppermute x1, waiting for transfers between devices: 0.01 us -> 13.8 us  [local(): from_right = lax.ppermute(weights, 'fs', ring(4, -1))]
    all_to_all x2 -> x1, starting transfers between devices: 11.2 us -> 3.54 us  [exchange(): lax.all_to_all(value, 'sp_1', split_axis=0, concat_axis=0, tiled=True)]
    pallas_call x5 -> x6, Pallas kernels: 24.3 us -> 18.1 us  [call(): pl.pallas_call(kernel, out_shape=shapes if many else shapes[0], in_specs=...]
    unnamed x36 -> x20, local copies, waits for them, and re-layouts: 4.23 us -> 0.61 us
    ppermute x2 -> x1, starting transfers between devices: 6.65 us -> 4.65 us  [local(): far = lax.ppermute(weights, 'fs', ring(4, 2))]
    slice x2 -> x0, local copies, waits for them, and re-layouts: 1.71 us -> none  [the longest x1 0.87 us: local(): far_a = lax.ppermute(from_left[:384], 'fs', ring(4, 1))]
  transfers between devices with their start and end apart: 8 -> 6, of which waited for: 2 -> 3; matrix products, arithmetic and copies ran while one was open for 5% -> 0% of each run, Pallas kernels for 18% -> 13%
where the time goes in v2:
time: 89.1 us; the launch traced here: 88.7 us
  blocking collectives  29.8 us (33%)
  starting transfers between devices  21.9 us (25%)
  Pallas kernels  18.1 us (20%)
  waiting for transfers between devices  15.6 us (18%)
  local copies, waits for them, and re-layouts  1.46 us (2%)
  other arithmetic  0.92 us (1%)
    all_to_all x1, blocking collectives, exchange(): lax.all_to_all(value, 'sp_1', split_axis=0, concat_axis=0, tiled=True)  29.8 us
    pallas_call x6, Pallas kernels, call(): pl.pallas_call(kernel, out_shape=shapes if many else shapes[0], in_specs=...  18.1 us
    ppermute x1, waiting for transfers between devices, local(): from_right = lax.ppermute(weights, 'fs', ring(4, -1))  13.8 us
    ppermute x1, starting transfers between devices, local(): other = lax.ppermute(got[:, STATE_ROWS:], 'tp', [(0, 1), (1, 0)])  5.9 us
    ppermute x1, starting transfers between devices, local(): far = lax.ppermute(weights, 'fs', ring(4, 2))  4.65 us
    all_to_all x1, starting transfers between devices, exchange(): lax.all_to_all(value, 'sp_1', split_axis=0, concat_axis=0, tiled=True)  3.54 us
    ppermute x1, starting transfers between devices, local(): from_right = lax.ppermute(weights, 'fs', ring(4, -1))  2.77 us
    ppermute x1, starting transfers between devices, local(): arrived = lax.ppermute(send, 'tp', [(0, 1), (1, 0)])  2.54 us
  transfers between devices with their start and end apart: 6, of which 3 were waited for; matrix products, arithmetic and copies ran while one was open for 0% of the time, Pallas kernels for 13%

profile of v2, /device:TPU:1, one launch (start us, length us, event | category | flops | bytes accessed | tf_op | source)
XLA Modules:
  0.0 88.7 jit_solution(5265179325082027570)
XLA Ops:
  0.6 4.0 %shard_map.158 = (bf16[8,432,128]{2,1,0:T(8,128)(2,1)}, bf16[768,512]{1,0:T(8,128)(2,1)}) custom-call(bf16[256,512]{1,0:T(8,128)(2,1)} %bitcast.18, bf16[256,512]{1,0:T(8,128)(2,1)} %bitcast.20, f32[2,512]{1,0:T(2,128)} %floor_ref.1, f32[4,256]{1,0:T(4,128)} %bitcast.24, bf16[256,256]{1,0:T(8,128)(2,1)} %bitcast.26, f32[1,256]{1,0:T(1,128)} %bitcast.29, ...), custom_call_target="tpu_custom_call" | custom-call | flops 536870912 | bytes 1048576 | tf_op jit(solution)/shard_map/pallas_call | solution.py:362
  4.6 29.8 %all_to_all.10.got_ref = bf16[8,432,128]{2,1,0:T(8,128)(2,1)S(1)} all-to-all(bf16[8,432,128]{2,1,0:T(8,128)(2,1)} %get-tuple-element.15), channel_id=1, replica_groups=mesh['sp_0'=8,'sp_1'=8,'fs'=4,'tp'=2] {'sp_1'}, dimensions={0} | all-to-all | bytes 1769472 | tf_op jit(solution)/shard_map/all_to_all | solution.py:387
  34.4 0.0 copy-start.9
  34.4 0.9 slice.4
  35.3 5.9 %collective-permute-start = (bf16[8,288,128]{2,1,0:T(8,128)(2,1)}, bf16[8,288,128]{2,1,0:T(8,128)(2,1)S(1)}, u32[]{:S(2)}, u32[]{:S(2)}) collective-permute-start(bf16[8,288,128]{2,1,0:T(8,128)(2,1)} %slice.4), channel_id=1, source_target_pairs={{0,1},{1,0},{2,3},{3,2},{4,5},{5,4},{6,7},{7,6},{8,9},{9,8},{10,11... | collective-permute-start | bytes 1769480 | tf_op jit(solution)/shard_map/ppermute | solution.py:461
  41.2 0.0 copy-done.9
  41.2 4.7 %collective-permute-start.3 = (bf16[768,512]{1,0:T(8,128)(2,1)S(1)}, bf16[768,512]{1,0:T(8,128)(2,1)}, u32[]{:S(2)}, u32[]{:S(2)}) collective-permute-start(bf16[768,512]{1,0:T(8,128)(2,1)S(1)} %copy-done.9), channel_id=1, source_target_pairs={{0,4},{2,6},{4,0},{6,2},{1,5},{3,7},{5,1},{7,3},{8,12},{10,14},{12... | collective-permute-start | bytes 2359304 | tf_op jit(solution)/shard_map/ppermute | solution.py:440
  45.9 2.8 %collective-permute-start.2 = (bf16[768,512]{1,0:T(8,128)(2,1)S(1)}, bf16[768,512]{1,0:T(8,128)(2,1)}, u32[]{:S(2)}, u32[]{:S(2)}) collective-permute-start(bf16[768,512]{1,0:T(8,128)(2,1)S(1)} %copy-done.9), channel_id=1, source_target_pairs={{0,6},{2,0},{4,2},{6,4},{1,7},{3,1},{5,3},{7,5},{8,14},{10,8},{12,... | collective-permute-start | bytes 2359304 | tf_op jit(solution)/shard_map/ppermute | solution.py:439
  48.6 2.5 %collective-permute-start.1 = (bf16[768,512]{1,0:T(8,128)(2,1)S(1)}, bf16[768,512]{1,0:T(8,128)(2,1)}, u32[]{:S(2)}, u32[]{:S(2)}) collective-permute-start(bf16[768,512]{1,0:T(8,128)(2,1)S(1)} %copy-done.9), channel_id=1, source_target_pairs={{0,2},{2,4},{4,6},{6,0},{1,3},{3,5},{5,7},{7,1},{8,10},{10,12},{12... | collective-permute-start | bytes 2359304 | tf_op jit(solution)/shard_map/ppermute | solution.py:438
  51.2 0.0 copy-start.3
  51.2 0.0 copy-start.5
  51.2 0.0 copy-start.6
  51.2 0.8 shard_map.162
  52.0 0.0 copy-start.1
  52.0 0.0 copy-start.2
  52.0 3.5 %all-to-all-start.1 = ((bf16[8,128,128]{2,1,0:T(8,128)(2,1)}), bf16[8,128,128]{2,1,0:T(8,128)(2,1)S(1)}, u32[]{:S(2)}, u32[]{:S(2)}) async-start(bf16[8,128,128]{2,1,0:T(8,128)(2,1)} %shard_map.162), calls=%async_computation.1 | async-start | bytes 524288 | tf_op jit(solution)/shard_map/all_to_all | solution.py:387
  55.5 0.0 copy-done.3
  55.5 0.0 copy-done.5
  55.5 0.0 copy-done.6
  55.5 0.0 copy-done.1
  55.5 0.0 copy-done.2
  55.6 0.0 copy-start
  55.6 5.6 %shard_map.160 = (f32[256,512]{1,0:T(8,128)}, bf16[2,256,512]{2,1,0:T(8,128)(2,1)}) custom-call(bf16[256,512]{1,0:T(8,128)(2,1)S(1)} %bitcast.22, bf16[256,512]{1,0:T(8,128)(2,1)S(1)} %bitcast.19, bf16[256,512]{1,0:T(8,128)(2,1)S(1)} %bitcast.21, f32[2,512]{1,0:T(2,128)S(1)} %copy-done.5, f32[4,256]{1,0:T(4,128)S(1)} %bitcast.25), custom_call_target="tpu_custom_call" | custom-call | flops 1073741824 | bytes 1048576 | tf_op jit(solution)/shard_map/pallas_call | solution.py:362
  61.1 0.0 copy-done
  61.2 0.0 copy-start.4
  61.2 0.0 copy-start.7
  61.2 0.0 copy-start.8
  61.2 0.5 shard_map.159
  61.7 0.0 collective-permute-done.other_ref
  61.7 0.4 copy-done.4
  62.1 0.1 copy-done.7
  62.2 0.1 copy-done.8
  62.2 4.7 %shard_map.161 = (bf16[256,256]{1,0:T(8,128)(2,1)S(1)}, f32[4,256]{1,0:T(4,128)}, f32[256,512]{1,0:T(8,128)S(1)}, bf16[2,256,512]{2,1,0:T(8,128)(2,1)S(1)}, f32[1,512]{1,0:T(1,128)S(1)}) custom-call(bf16[256,384]{1,0:T(8,128)(2,1)S(1)} %bitcast.23, bf16[8,288,128]{2,1,0:T(8,128)(2,1)S(1)} %collective-permute-done.other_ref, ...), custom_call_target="tpu_custom_call" | custom-call | flops 2147483648 | bytes 1048576 | tf_op jit(solution)/shard_map/pallas_call | solution.py:362
  66.9 0.0 collective-permute-done.3.far_hbm
  66.9 13.8 %collective-permute-done.2.right_hbm = bf16[768,512]{1,0:T(8,128)(2,1)} collective-permute-done((bf16[768,512]{1,0:T(8,128)(2,1)S(1)}, bf16[768,512]{1,0:T(8,128)(2,1)}, u32[]{:S(2)}, u32[]{:S(2)}) %collective-permute-start.2) | collective-permute-done | bytes 786464 | tf_op jit(solution)/shard_map/ppermute | solution.py:439
  80.8 0.2 collective-permute-done.1.left_hbm
  81.0 0.0 all-to-all-done.1.state_ref
  81.0 2.7 %shard_map.163 = (bf16[128,2048]{1,0:T(8,128)(2,1)S(1)}, bf16[128,2048]{1,0:T(8,128)(2,1)S(1)}) custom-call(f32[256,512]{1,0:T(8,128)S(1)} %get-tuple-element.20.local_ref, bf16[2,256,512]{2,1,0:T(8,128)(2,1)S(1)} %get-tuple-element.21.damped_ref, bf16[8,128,128]{2,1,0:T(8,128)(2,1)S(1)} %all-to-all-done.1.state_ref, ...), custom_call_target="tpu_custom_call" | custom-call | flops 1073741824 | bytes 1048576 | tf_op jit(solution)/shard_map/pallas_call | solution.py:362
  83.7 2.5 %collective-permute-start.4 = (bf16[128,2048]{1,0:T(8,128)(2,1)S(1)}, bf16[128,2048]{1,0:T(8,128)(2,1)S(1)}, u32[]{:S(2)}, u32[]{:S(2)}) collective-permute-start(bf16[128,2048]{1,0:T(8,128)(2,1)S(1)} %get-tuple-element.26), channel_id=1, source_target_pairs={{0,1},{1,0},{2,3},{3,2},{4,5},{5,4},{6,7},{7,6},{8,9},{9,8},{10,11... | collective-permute-start | bytes 1572872 | tf_op jit(solution)/shard_map/ppermute | solution.py:501
  86.2 1.5 %collective-permute-done.4 = bf16[128,2048]{1,0:T(8,128)(2,1)S(1)} collective-permute-done((bf16[128,2048]{1,0:T(8,128)(2,1)S(1)}, bf16[128,2048]{1,0:T(8,128)(2,1)S(1)}, u32[]{:S(2)}, u32[]{:S(2)}) %collective-permute-start.4) | collective-permute-done | bytes 524320 | tf_op jit(solution)/shard_map/ppermute | solution.py:501
  87.7 0.9 %fusion = bf16[1,128,2048]{2,1,0:T(8,128)(2,1)} fusion(bf16[128,2048]{1,0:T(8,128)(2,1)S(1)} %collective-permute-done.4, bf16[128,2048]{1,0:T(8,128)(2,1)S(1)} %get-tuple-element.25), kind=kLoop, calls=%fused_computation.1 | loop fusion | flops 1048576 | bytes 1572864 | tf_op jit(solution)/shard_map/broadcast_in_dim | solution.py:503
Async XLA Ops:
  34.4 6.8 %copy-start.9 = (bf16[768,512]{1,0:T(8,128)(2,1)S(1)}, bf16[768,512]{1,0:T(8,128)(2,1)}, u32[]{:S(2)}) copy-start(bf16[768,512]{1,0:T(8,128)(2,1)} %get-tuple-element.24.own_hbm) | copy-start | bytes 2359300
  35.3 26.4 %collective-permute-start = (bf16[8,288,128]{2,1,0:T(8,128)(2,1)}, bf16[8,288,128]{2,1,0:T(8,128)(2,1)S(1)}, u32[]{:S(2)}, u32[]{:S(2)}) collective-permute-start(bf16[8,288,128]{2,1,0:T(8,128)(2,1)} %slice.4), channel_id=1, source_target_pairs={{0,1},{1,0},{2,3},{3,2},{4,5},{5,4},{6,7},{7,6},{8,9},{9,8},{10,11... | collective-permute-start | bytes 1769480 | tf_op jit(solution)/shard_map/ppermute | solution.py:461
  41.2 25.7 %collective-permute-start.3 = (bf16[768,512]{1,0:T(8,128)(2,1)S(1)}, bf16[768,512]{1,0:T(8,128)(2,1)}, u32[]{:S(2)}, u32[]{:S(2)}) collective-permute-start(bf16[768,512]{1,0:T(8,128)(2,1)S(1)} %copy-done.9), channel_id=1, source_target_pairs={{0,4},{2,6},{4,0},{6,2},{1,5},{3,7},{5,1},{7,3},{8,12},{10,14},{12... | collective-permute-start | bytes 2359304 | tf_op jit(solution)/shard_map/ppermute | solution.py:440
  45.9 34.9 %collective-permute-start.2 = (bf16[768,512]{1,0:T(8,128)(2,1)S(1)}, bf16[768,512]{1,0:T(8,128)(2,1)}, u32[]{:S(2)}, u32[]{:S(2)}) collective-permute-start(bf16[768,512]{1,0:T(8,128)(2,1)S(1)} %copy-done.9), channel_id=1, source_target_pairs={{0,6},{2,0},{4,2},{6,4},{1,7},{3,1},{5,3},{7,5},{8,14},{10,8},{12,... | collective-permute-start | bytes 2359304 | tf_op jit(solution)/shard_map/ppermute | solution.py:439
  48.6 32.4 %collective-permute-start.1 = (bf16[768,512]{1,0:T(8,128)(2,1)S(1)}, bf16[768,512]{1,0:T(8,128)(2,1)}, u32[]{:S(2)}, u32[]{:S(2)}) collective-permute-start(bf16[768,512]{1,0:T(8,128)(2,1)S(1)} %copy-done.9), channel_id=1, source_target_pairs={{0,2},{2,4},{4,6},{6,0},{1,3},{3,5},{5,7},{7,1},{8,10},{10,12},{12... | collective-permute-start | bytes 2359304 | tf_op jit(solution)/shard_map/ppermute | solution.py:438
  51.2 4.4 %copy-start.3 = (bf16[1,256,512]{2,1,0:T(8,128)(2,1)S(1)}, bf16[1,256,512]{2,1,0:T(8,128)(2,1)}, u32[]{:S(2)}) copy-start(bf16[1,256,512]{2,1,0:T(8,128)(2,1)} %param.15) | copy-start | bytes 786436
  51.2 4.4 %copy-start.5 = (f32[2,512]{1,0:T(2,128)S(1)}, f32[2,512]{1,0:T(2,128)}, u32[]{:S(2)}) copy-start(f32[2,512]{1,0:T(2,128)} %floor_ref.1) | copy-start | bytes 12292
  51.2 4.4 %copy-start.6 = (f32[1,256,4]{1,2,0:T(4,128)S(1)}, f32[1,256,4]{1,2,0:T(4,128)}, u32[]{:S(2)}) copy-start(f32[1,256,4]{1,2,0:T(4,128)} %param.19) | copy-start | bytes 12292
  52.0 3.6 %copy-start.1 = (bf16[1,256,512]{2,1,0:T(8,128)(2,1)S(1)}, bf16[1,256,512]{2,1,0:T(8,128)(2,1)}, u32[]{:S(2)}) copy-start(bf16[1,256,512]{2,1,0:T(8,128)(2,1)} %param.16) | copy-start | bytes 786436
  52.0 3.6 %copy-start.2 = (bf16[1,256,512]{2,1,0:T(8,128)(2,1)S(1)}, bf16[1,256,512]{2,1,0:T(8,128)(2,1)}, u32[]{:S(2)}) copy-start(bf16[1,256,512]{2,1,0:T(8,128)(2,1)} %param.17) | copy-start | bytes 786436
  52.0 29.1 %all-to-all-start.1 = ((bf16[8,128,128]{2,1,0:T(8,128)(2,1)}), bf16[8,128,128]{2,1,0:T(8,128)(2,1)S(1)}, u32[]{:S(2)}, u32[]{:S(2)}) async-start(bf16[8,128,128]{2,1,0:T(8,128)(2,1)} %shard_map.162), calls=%async_computation.1 | async-start | bytes 524288 | tf_op jit(solution)/shard_map/all_to_all | solution.py:387
  55.6 5.6 %copy-start = (bf16[256,1024]{1,0:T(8,128)(2,1)S(1)}, bf16[256,1024]{1,0:T(8,128)(2,1)}, u32[]{:S(2)}) copy-start(bf16[256,1024]{1,0:T(8,128)(2,1)} %up_ref.3) | copy-start | bytes 1572868
  61.2 0.9 %copy-start.4 = (bf16[1,256,384]{2,1,0:T(8,128)(2,1)S(1)}, bf16[1,256,384]{2,1,0:T(8,128)(2,1)}, u32[]{:S(2)}) copy-start(bf16[1,256,384]{2,1,0:T(8,128)(2,1)} %param.21) | copy-start | bytes 589828
  61.2 1.0 %copy-start.7 = (f32[16,2048]{1,0:T(8,128)S(1)}, f32[16,2048]{1,0:T(8,128)}, u32[]{:S(2)}) copy-start(f32[16,2048]{1,0:T(8,128)} %constant.5.clone.sin_hbm.sin_ref) | copy-start | bytes 393220
  61.2 1.0 %copy-start.8 = (f32[16,2048]{1,0:T(8,128)S(1)}, f32[16,2048]{1,0:T(8,128)}, u32[]{:S(2)}) copy-start(f32[16,2048]{1,0:T(8,128)} %constant.4.clone.cos_hbm.cos_ref) | copy-start | bytes 393220
  83.7 4.1 %collective-permute-start.4 = (bf16[128,2048]{1,0:T(8,128)(2,1)S(1)}, bf16[128,2048]{1,0:T(8,128)(2,1)S(1)}, u32[]{:S(2)}, u32[]{:S(2)}) collective-permute-start(bf16[128,2048]{1,0:T(8,128)(2,1)S(1)} %get-tuple-element.26), channel_id=1, source_target_pairs={{0,1},{1,0},{2,3},{3,2},{4,5},{5,4},{6,7},{7,6},{8,9},{9,8},{10,11... | collective-permute-start | bytes 1572872 | tf_op jit(solution)/shard_map/ppermute | solution.py:501

commit v3 on v2

--- a/solution.py
+++ b/solution.py
@@ -18,8 +18,8 @@
 TOK = 256
 HALF = 128
 SEQ_DEV = 8
-STATE_ROWS = 144
-KV_ROWS = 288
+STATE_ROWS = 136
+KV_ROWS = 144
 CHUNK_ROWS = STATE_ROWS + KV_ROWS
 SP = ("sp_0", "sp_1")
 SP_TP = ("sp_0", "sp_1", "tp")
@@ -82,10 +82,9 @@
 
 def send_kernel(
     logit_hbm, value_hbm, floor_hbm, extra_hbm, lat_hbm, gain_hbm, key_hbm, cos_hbm, sin_hbm,
-    upper_hbm, lower_hbm,
-    out_hbm, weight_hbm,
+    out_hbm,
     logit_ref, value_ref, floor_ref, extra_ref, lat_ref, gain_ref, key_ref, cos_ref, sin_ref,
-    state_ref, kv_ref, weight_ref, in_sems, kv_sems, state_sems, weight_sem,
+    state_ref, kv_ref, in_sems, kv_sems, state_sems,
 ):
     tp, place = lax.axis_index("tp"), lax.axis_index("sp_1")
     mine = pl.ds(pl.multiple_of(tp * HALF, HALF), HALF)
@@ -102,8 +101,6 @@
             (extra_hbm, extra_ref),
             (floor_hbm, floor_ref),
             (value_hbm, value_ref),
-            (upper_hbm, weight_ref.at[0:512, :]),
-            (lower_hbm, weight_ref.at[512:768, :]),
         ],
     )
     for load in loads[:5]:
@@ -115,27 +112,21 @@
     cos, sin = cos_ref[...], sin_ref[...]
     turned = jnp.concatenate(
         [key[:16] * cos - key[16:] * sin, key[:16] * sin + key[16:] * cos], axis=0
-    ).astype(bf16)
-    kv_ref[0:128, :] = normed[:, :128]
-    kv_ref[128:256, :] = normed[:, 128:]
-    kv_ref[256:KV_ROWS, :] = turned
+    )
+    for p in range(2):
+        kv_ref[p, 0:128, :] = normed[:, p * 128 : (p + 1) * 128]
+        kv_ref[p, 128:KV_ROWS, :] = turned[p * 16 : (p + 1) * 16].astype(bf16)
     stores = start_all(
         kv_sems,
-        [(kv_ref, out_hbm.at[q, STATE_ROWS:CHUNK_ROWS, :]) for q in range(SEQ_DEV)],
-    )
-    for load in loads[5:9]:
+        [(kv_ref.at[q % 2], out_hbm.at[q, STATE_ROWS:CHUNK_ROWS, :]) for q in range(SEQ_DEV)],
+    )
+    for load in loads[5:]:
         load.wait()
     rows = iota2((TOK, TOK), 0)
     cols = iota2((TOK, TOK), 1)
     after = (cols > rows).astype(f32).astype(bf16)
     before = (cols < rows).astype(f32).astype(bf16)
     for pair in range(HEADS // 2):
-        if pair == 1:
-            for load in loads[9:]:
-                load.wait()
-            weight_store = pltpu.make_async_copy(weight_ref, weight_hbm, weight_sem)
-            weight_store.start()
-            stores.append(weight_store)
         lanes = slice(pair * 2 * DK, (pair + 1) * 2 * DK)
         closed = shut(logit_ref[:, lanes].astype(f32))
         extra = head_extra(extra_ref, 2 * pair, 2)
@@ -231,26 +222,38 @@
             carried = carried * decay + got_ref[j, 0:DK, :].astype(f32)
 
 
-def unpack_rope(rope_ref, ref, base):
+def unpack_rope(rope_ref, ref):
+    even = lax.axis_index("sp_1") % 2 == 0
     for j in range(SEQ_DEV):
-        turned = ref[j, base + 256 : base + 288, :].astype(f32)
+        one = ref[j, 128:KV_ROWS, :].astype(f32)
+        two = ref[j, KV_ROWS + 128 : 2 * KV_ROWS, :].astype(f32)
         rope_ref[j * 128 : j * 128 + 128, :] = jnp.transpose(
-            jnp.concatenate([jnp.zeros((NOPE, 128), f32), turned, jnp.zeros((32, 128), f32)], axis=0)
+            jnp.concatenate(
+                [
+                    jnp.zeros((NOPE, 128), f32),
+                    jnp.where(even, one, two),
+                    jnp.where(even, two, one),
+                    jnp.zeros((32, 128), f32),
+                ],
+                axis=0,
+            )
         ).astype(bf16)
 
 
-def expand(ex_ref, ref, base, up_ref):
-    up = up_ref[:, pl.ds(pl.multiple_of(lax.axis_index("tp") * HEADS * 128, HEADS * 128), HEADS * 128)]
+def expand(ex_ref, ref, up_ref):
+    columns = pl.ds(pl.multiple_of(lax.axis_index("tp") * HEADS * 128, HEADS * 128), HEADS * 128)
+    odd = lax.axis_index("sp_1") % 2
+    up = jnp.concatenate(
+        [up_ref[pl.ds(pl.multiple_of(p * 128, 128), 128), columns] for p in (odd, 1 - odd)], axis=0
+    )
     for j in range(SEQ_DEV):
-        lat = jnp.concatenate(
-            [ref[j, base : base + 128, :], ref[j, base + 128 : base + 256, :]], axis=1
-        )
+        lat = jnp.concatenate([ref[j, 0:128, :], ref[j, KV_ROWS : KV_ROWS + 128, :]], axis=1)
         ex_ref[j * 128 : j * 128 + 128, :] = dot(lat, up).astype(bf16)
 
 
-def expand_kernel(got_ref, up_ref, ex_ref, rope_ref):
-    unpack_rope(rope_ref, got_ref, STATE_ROWS)
-    expand(ex_ref, got_ref, STATE_ROWS, up_ref)
+def expand_kernel(pair_ref, up_ref, ex_ref, rope_ref):
+    unpack_rope(rope_ref, pair_ref)
+    expand(ex_ref, pair_ref, up_ref)
 
 
 def attend_kernel(
@@ -262,8 +265,8 @@
     loads = start_all(
         sems, [(local_hbm, local_ref), (damped_hbm, damped_ref), (gain_hbm, gain_ref)]
     )
-    unpack_rope(rope_ref, other_ref, 0)
-    expand(ex_ref, other_ref, 0, up_ref)
+    unpack_rope(rope_ref, other_ref)
+    expand(ex_ref, other_ref, up_ref)
     spot = pl.ds(pl.multiple_of(lax.axis_index("sp_1") * TOK, TOK), TOK)
     cos, sin = cos_ref[:, spot], sin_ref[:, spot]
     nothing = jnp.zeros((NOPE, TOK), f32)
@@ -312,14 +315,19 @@
 
 
 def finish_kernel(
-    local_ref, damped_ref, state_ref, gain_ref, att_ref, own_hbm, left_hbm, right_hbm, far_hbm,
+    local_ref, damped_ref, state_ref, gain_ref, att_ref, far_ref, top_hbm, low_hbm, left_hbm, right_hbm,
     send_ref, keep_ref,
     weight_ref, act_ref, sems,
 ):
     tp, column = lax.axis_index("tp"), lax.axis_index("fs")
     loads = start_all(
         sems,
-        [(ref, weight_ref.at[i]) for i, ref in enumerate((own_hbm, left_hbm, right_hbm, far_hbm))],
+        [
+            (top_hbm, weight_ref.at[0, 0:512, :]),
+            (low_hbm, weight_ref.at[0, 512:768, :]),
+            (left_hbm, weight_ref.at[1]),
+            (right_hbm, weight_ref.at[2]),
+        ],
     )
     for part in range(2):
         start = jnp.where(tp == part, HALF, 0)
@@ -327,19 +335,18 @@
         to = slice(part * HALF, (part + 1) * HALF)
         for h in range(HEADS):
             lanes = slice(h * DK, (h + 1) * DK)
-            o = (
-                local_ref[at, lanes]
-                + dot(damped_ref[0, at, lanes], state_ref[h], NT)
-                + dot(damped_ref[1, at, lanes], state_ref[HEADS + h], NT)
-            )
+            damped = jnp.concatenate([damped_ref[0, at, lanes], damped_ref[1, at, lanes]], axis=1)
+            state = jnp.concatenate([state_ref[h], state_ref[HEADS + h]], axis=1)
+            o = local_ref[at, lanes] + dot(damped, state, NT)
             mean = jnp.sum(o * o, axis=1, keepdims=True) * (1.0 / DK)
             act_ref[to, lanes] = (o * lax.rsqrt(mean + EPS) * gain_ref[:, lanes]).astype(bf16)
         act_ref[to, HEADS * DK :] = att_ref[at, :]
     act = act_ref[...]
     for i in range(4):
-        loads[i].wait()
-        got = dot(act, weight_ref[i]).astype(bf16)
-        lanes = pl.ds(pl.multiple_of(((column + (0, 3, 1, 2)[i]) % 4) * 512, 512), 512)
+        for load in ((), loads[:2], loads[2:3], loads[3:])[i]:
+            load.wait()
+        got = dot(act, far_ref[...] if i == 0 else weight_ref[i - 1]).astype(bf16)
+        lanes = pl.ds(pl.multiple_of(((column + (2, 0, 3, 1)[i]) % 4) * 512, 512), 512)
         send_ref[:, lanes] = got[:HALF]
         keep_ref[:, lanes] = got[HALF:]
 
@@ -352,11 +359,13 @@
         pltpu.with_memory_space_constraint(a, pltpu.HBM) if c == "h" else a for c, a in zip(ins, args)
     ]
     many = isinstance(outs, tuple)
-    spaces = [
-        pltpu.HBM if isinstance(o, HbmOut) else pltpu.VMEM for o in (outs if many else (outs,))
-    ]
+    listed = outs if many else (outs,)
+    spaces = [pltpu.HBM if type(o) is HbmOut else pltpu.VMEM for o in listed]
     shapes = tuple(
-        pltpu.HBM(o.dims, o.dtype) if isinstance(o, HbmOut) else o for o in (outs if many else (outs,))
+        pltpu.HBM(o.dims, o.dtype)
+        if type(o) is HbmOut
+        else o
+        for o in listed
     )
     specs = tuple(pl.BlockSpec(memory_space=space) for space in spaces)
     return pl.pallas_call(
@@ -377,6 +386,9 @@
 
 def shape(dims, dtype):
     return jax.ShapeDtypeStruct(dims, dtype)
+
+
+NEXT = [(i, (i + (1 if i % 2 else 7)) % 8) for i in range(8)]
 
 
 def ring(n, step):
@@ -406,13 +418,12 @@
     logits, values = forget_logits[0], recurrent_value[0]
     extra = jnp.swapaxes(extra_log_decay[0], 0, 1)
 
-    sent, weights = call(
+    sent = call(
         send_kernel,
-        "h" * 11,
-        (HbmOut((SEQ_DEV, CHUNK_ROWS, DK), bf16), HbmOut((768, 512), bf16)),
+        "h" * 9,
+        HbmOut((SEQ_DEV, CHUNK_ROWS, DK), bf16),
         logits, values, forget_floor, extra, latent[0], latent_norm_gain.reshape(1, RANK),
         jnp.swapaxes(rotary_key[0], 0, 1), cos_table, sin_table,
-        recurrent_output_weight, attention_output_weight,
         scratch=(
             pltpu.VMEM((TOK, HEADS * DK), bf16),
             pltpu.VMEM((TOK, HEADS * DK), bf16),
@@ -424,17 +435,16 @@
             pltpu.VMEM((16, HALF), f32),
             pltpu.VMEM((16, HALF), f32),
             pltpu.VMEM((2 * HEADS, STATE_ROWS, DK), bf16),
-            pltpu.VMEM((KV_ROWS, DK), bf16),
-            pltpu.VMEM((768, 512), bf16),
-            pltpu.SemaphoreType.DMA((11,)),
+            pltpu.VMEM((2, KV_ROWS, DK), bf16),
+            pltpu.SemaphoreType.DMA((9,)),
             pltpu.SemaphoreType.DMA((SEQ_DEV,)),
             pltpu.SemaphoreType.DMA((2 * HEADS,)),
-            pltpu.SemaphoreType.DMA,
         ),
         flops=1 << 29, mib=14,
     )
     got = exchange(sent)
 
+    weights = jnp.concatenate([recurrent_output_weight, attention_output_weight], axis=0)
     from_left = lax.ppermute(weights, "fs", ring(4, 1))
     from_right = lax.ppermute(weights, "fs", ring(4, -1))
     far = lax.ppermute(weights, "fs", ring(4, 2))
@@ -458,12 +468,14 @@
     )
     states = exchange(scanned)
 
-    other = lax.ppermute(got[:, STATE_ROWS:], "tp", [(0, 1), (1, 0)])
+    mine = got[:, STATE_ROWS:]
+    pair = jnp.concatenate([mine, lax.ppermute(mine, "sp_1", NEXT)], axis=1)
+    other = lax.ppermute(pair, "tp", [(0, 1), (1, 0)])
     keys = SEQ_DEV * HALF
     ex_mine, rope_mine = call(
         expand_kernel, "vv",
         (shape((keys, HEADS * 128), bf16), shape((keys, 128), bf16)),
-        got, latent_up_weight,
+        pair, latent_up_weight,
         flops=1 << 28, mib=12,
     )
     attended, log_weight, local_out, damped, gain = call(
@@ -488,11 +500,12 @@
 
     send, keep = call(
         finish_kernel,
-        "v" * 5 + "h" * 4,
+        "v" * 6 + "hhhh",
         (shape((HALF, 2048), bf16), shape((HALF, 2048), bf16)),
-        local_out, damped, states, gain, attended, weights, from_left, from_right, far,
+        local_out, damped, states, gain, attended, far,
+        recurrent_output_weight, attention_output_weight, from_left, from_right,
         scratch=(
-            pltpu.VMEM((4, 768, 512), bf16),
+            pltpu.VMEM((3, 768, 512), bf16),
             pltpu.VMEM((TOK, 768), bf16),
             pltpu.SemaphoreType.DMA((4,)),
         ),

time: 89.1 us -> 92.7 us (1.040)
  blocking collectives: 29.8 us -> 23.2 us
  starting transfers between devices: 21.9 us -> 26.9 us
  waiting for transfers between devices: 15.6 us -> 20.4 us
    ppermute x1, waiting for transfers between devices: 13.8 us -> 0.01 us  [local(): from_right = lax.ppermute(weights, 'fs', ring(4, -1))]
    ppermute x1, waiting for transfers between devices: 0.25 us -> 13 us  [local(): from_left = lax.ppermute(weights, 'fs', ring(4, 1))]
    all_to_all x1, blocking collectives: 29.8 us -> 23.2 us  [exchange(): lax.all_to_all(value, 'sp_1', split_axis=0, concat_axis=0, tiled=True)]
    ppermute x1 -> x2, waiting for transfers between devices: 0.01 us -> 5.89 us  [the longest x1 5.89 us: local(): pair = jnp.concatenate([mine, lax.ppermute(mine, 'sp_1', NEXT)], axis=1)]
    ppermute x1 -> x2, starting transfers between devices: 5.9 us -> 9.35 us  [the longest x1 7.29 us: local(): other = lax.ppermute(pair, 'tp', [(0, 1), (1, 0)])]
    ppermute x1, starting transfers between devices: 2.77 us -> 4.29 us  [local(): from_right = lax.ppermute(weights, 'fs', ring(4, -1))]
  transfers between devices with their start and end apart: 6 -> 7, of which waited for: 3 -> 3; matrix products, arithmetic and copies ran while one was open for 0% -> 2% of each run, Pallas kernels for 13% -> 13%
where the time goes in v3:
time: 92.7 us; the launch traced here: 92.1 us
  starting transfers between devices  26.9 us (29%)
  blocking collectives  23.2 us (25%)
  waiting for transfers between devices  20.4 us (22%)
  Pallas kernels  17.6 us (19%)
  local copies, waits for them, and re-layouts  2.21 us (2%)
  other arithmetic  0.96 us (1%)
    all_to_all x1, blocking collectives, exchange(): lax.all_to_all(value, 'sp_1', split_axis=0, concat_axis=0, tiled=True)  23.2 us
    pallas_call x6, Pallas kernels, call(): pl.pallas_call(kernel, out_shape=shapes if many else shapes[0], in_specs=...  17.6 us
    ppermute x1, waiting for transfers between devices, local(): from_left = lax.ppermute(weights, 'fs', ring(4, 1))  13 us
    ppermute x1, starting transfers between devices, local(): other = lax.ppermute(pair, 'tp', [(0, 1), (1, 0)])  7.29 us
    ppermute x1, waiting for transfers between devices, local(): pair = jnp.concatenate([mine, lax.ppermute(mine, 'sp_1', NEXT)], axis=1)  5.89 us
    ppermute x1, starting transfers between devices, local(): far = lax.ppermute(weights, 'fs', ring(4, 2))  4.94 us
    ppermute x1, starting transfers between devices, local(): from_right = lax.ppermute(weights, 'fs', ring(4, -1))  4.29 us
    all_to_all x1, starting transfers between devices, exchange(): lax.all_to_all(value, 'sp_1', split_axis=0, concat_axis=0, tiled=True)  3.41 us
  transfers between devices with their start and end apart: 7, of which 3 were waited for; matrix products, arithmetic and copies ran while one was open for 2% of the time, Pallas kernels for 13%

profile of v3, /device:TPU:1, one launch (start us, length us, event | category | flops | bytes accessed | tf_op | source)
XLA Modules:
  0.0 92.1 jit_solution(14030690417655851145)
XLA Ops:
  0.6 3.5 %shard_map.158 = bf16[8,280,128]{2,1,0:T(8,128)(2,1)} custom-call(bf16[256,512]{1,0:T(8,128)(2,1)} %bitcast.18, bf16[256,512]{1,0:T(8,128)(2,1)} %bitcast.20, f32[2,512]{1,0:T(2,128)} %floor_ref.1, f32[4,256]{1,0:T(4,128)} %bitcast.24, bf16[256,256]{1,0:T(8,128)(2,1)} %bitcast.26, f32[1,256]{1,0:T(1,128)} %bitcast.29, bf16[32,256]{1,0:T(8,128)(2,1)} %bitcast.27, ...), custom_call_target="tpu_custom_call" | custom-call | flops 536870912 | bytes 1048576 | tf_op jit(solution)/shard_map/pallas_call | solution.py:371
  4.1 0.0 copy-start.9
  4.1 23.2 %all_to_all.10.got_ref = bf16[8,280,128]{2,1,0:T(8,128)(2,1)S(1)} all-to-all(bf16[8,280,128]{2,1,0:T(8,128)(2,1)} %shard_map.158), channel_id=1, replica_groups=mesh['sp_0'=8,'sp_1'=8,'fs'=4,'tp'=2] {'sp_1'}, dimensions={0} | all-to-all | bytes 1146880 | tf_op jit(solution)/shard_map/all_to_all | solution.py:399
  27.3 0.0 copy-start.10
  27.3 2.1 %collective-permute-start = (bf16[8,144,128]{2,1,0:T(8,128)(2,1)S(1)}, bf16[8,144,128]{2,1,0:T(8,128)(2,1)S(1)}, u32[]{:S(2)}, u32[]{:S(2)}) collective-permute-start(bf16[8,144,128]{2,1,0:T(8,128)(2,1)S(1)} %slice.4), channel_id=1, source_target_pairs={{0,56},{8,16},{16,8},{24,32},{32,24},{40,48},{48,40},{56,0},{1,57}... | collective-permute-start | bytes 884744 | tf_op jit(solution)/shard_map/ppermute | solution.py:472
  29.4 0.0 copy-done.9
  29.4 0.8 constant_dynamic-update-slice_fusion.1
  30.2 5.9 %collective-permute-done = bf16[8,144,128]{2,1,0:T(8,128)(2,1)S(1)} collective-permute-done((bf16[8,144,128]{2,1,0:T(8,128)(2,1)S(1)}, bf16[8,144,128]{2,1,0:T(8,128)(2,1)S(1)}, u32[]{:S(2)}, u32[]{:S(2)}) %collective-permute-start) | collective-permute-done | bytes 294944 | tf_op jit(solution)/shard_map/ppermute | solution.py:472
  36.2 0.0 copy-start.1
  36.2 0.0 copy-start.2
  36.2 0.0 copy-start.3
  36.2 0.0 copy-start.5
  36.2 0.0 copy-start.6
  36.2 7.3 %collective-permute-start.1 = (bf16[8,288,128]{2,1,0:T(8,128)(2,1)S(1)}, bf16[8,288,128]{2,1,0:T(8,128)(2,1)S(1)}, u32[]{:S(2)}, u32[]{:S(2)}) collective-permute-start(bf16[8,288,128]{2,1,0:T(8,128)(2,1)S(1)} %pad_maximum_fusion.pair_ref), channel_id=1, source_target_pairs={{0,1},{1,0},{2,3},{3,2},{4,5},{5,4},{6,7},{7,6},{8,9},{9,8},{10,11... | collective-permute-start | bytes 1769480 | tf_op jit(solution)/shard_map/ppermute | solution.py:473
  43.5 0.0 copy-done.10
  43.5 0.7 constant_dynamic-update-slice_fusion
  44.3 4.9 %collective-permute-start.2 = (bf16[768,512]{1,0:T(8,128)(2,1)}, bf16[768,512]{1,0:T(8,128)(2,1)S(1)}, u32[]{:S(2)}, u32[]{:S(2)}) collective-permute-start(bf16[768,512]{1,0:T(8,128)(2,1)} %constant_dynamic-update-slice_fusion), channel_id=1, source_target_pairs={{0,4},{2,6},{4,0},{6,2},{1,5},{3,7},{5,1},{7,3},{8,12},{10,14},{12... | collective-permute-start | bytes 2359304 | tf_op jit(solution)/shard_map/ppermute | solution.py:450
  49.2 2.2 %collective-permute-start.3 = (bf16[768,512]{1,0:T(8,128)(2,1)}, bf16[768,512]{1,0:T(8,128)(2,1)}, u32[]{:S(2)}, u32[]{:S(2)}) collective-permute-start(bf16[768,512]{1,0:T(8,128)(2,1)} %constant_dynamic-update-slice_fusion), channel_id=1, source_target_pairs={{0,2},{2,4},{4,6},{6,0},{1,3},{3,5},{5,7},{7,1},{8,10},{10,12},{12... | collective-permute-start | bytes 2359304 | tf_op jit(solution)/shard_map/ppermute | solution.py:448
  51.4 4.3 %collective-permute-start.4 = (bf16[768,512]{1,0:T(8,128)(2,1)}, bf16[768,512]{1,0:T(8,128)(2,1)}, u32[]{:S(2)}, u32[]{:S(2)}) collective-permute-start(bf16[768,512]{1,0:T(8,128)(2,1)} %constant_dynamic-update-slice_fusion), channel_id=1, source_target_pairs={{0,6},{2,0},{4,2},{6,4},{1,7},{3,1},{5,3},{7,5},{8,14},{10,8},{12,... | collective-permute-start | bytes 2359304 | tf_op jit(solution)/shard_map/ppermute | solution.py:449
  55.7 0.8 shard_map.162
  56.5 3.4 %all-to-all-start.1 = ((bf16[8,128,128]{2,1,0:T(8,128)(2,1)}), bf16[8,128,128]{2,1,0:T(8,128)(2,1)S(1)}, u32[]{:S(2)}, u32[]{:S(2)}) async-start(bf16[8,128,128]{2,1,0:T(8,128)(2,1)} %shard_map.162), calls=%async_computation.1 | async-start | bytes 524288 | tf_op jit(solution)/shard_map/all_to_all | solution.py:399
  59.9 0.0 copy-done.1
  59.9 0.0 copy-done.2
  59.9 0.0 copy-done.3
  60.0 0.0 copy-done.5
  60.0 0.0 copy-done.6
  60.0 0.0 copy-start
  60.0 5.6 %shard_map.160 = (f32[256,512]{1,0:T(8,128)}, bf16[2,256,512]{2,1,0:T(8,128)(2,1)}) custom-call(bf16[256,512]{1,0:T(8,128)(2,1)S(1)} %bitcast.22, bf16[256,512]{1,0:T(8,128)(2,1)S(1)} %bitcast.19, bf16[256,512]{1,0:T(8,128)(2,1)S(1)} %bitcast.21, f32[2,512]{1,0:T(2,128)S(1)} %copy-done.5, f32[4,256]{1,0:T(4,128)S(1)} %bitcast.25), custom_call_target="tpu_custom_call" | custom-call | flops 1073741824 | bytes 1048576 | tf_op jit(solution)/shard_map/pallas_call | solution.py:371
  65.6 0.0 copy-done
  65.6 0.0 copy-start.4
  65.6 0.0 copy-start.7
  65.6 0.0 copy-start.8
  65.6 0.5 shard_map.159
  66.1 0.0 collective-permute-done.1.other_ref
  66.1 0.4 copy-done.4
  66.5 0.1 copy-done.7
  66.6 0.1 copy-done.8
  66.7 4.7 %shard_map.161 = (bf16[256,256]{1,0:T(8,128)(2,1)S(1)}, f32[4,256]{1,0:T(4,128)}, f32[256,512]{1,0:T(8,128)S(1)}, bf16[2,256,512]{2,1,0:T(8,128)(2,1)S(1)}, f32[1,512]{1,0:T(1,128)S(1)}) custom-call(bf16[256,384]{1,0:T(8,128)(2,1)S(1)} %bitcast.23, bf16[8,288,128]{2,1,0:T(8,128)(2,1)S(1)} %collective-permute-done.1.other_ref, ...), custom_call_target="tpu_custom_call" | custom-call | flops 2147483648 | bytes 1048576 | tf_op jit(solution)/shard_map/pallas_call | solution.py:371
  71.4 0.0 collective-permute-done.2.far_ref
  71.4 13.0 %collective-permute-done.3.left_hbm = bf16[768,512]{1,0:T(8,128)(2,1)} collective-permute-done((bf16[768,512]{1,0:T(8,128)(2,1)}, bf16[768,512]{1,0:T(8,128)(2,1)}, u32[]{:S(2)}, u32[]{:S(2)}) %collective-permute-start.3) | collective-permute-done | bytes 786464 | tf_op jit(solution)/shard_map/ppermute | solution.py:448
  84.4 0.0 collective-permute-done.4.right_hbm
  84.4 0.0 all-to-all-done.1.state_ref
  84.4 2.6 %shard_map.163 = (bf16[128,2048]{1,0:T(8,128)(2,1)S(1)}, bf16[128,2048]{1,0:T(8,128)(2,1)S(1)}) custom-call(f32[256,512]{1,0:T(8,128)S(1)} %get-tuple-element.17.local_ref, bf16[2,256,512]{2,1,0:T(8,128)(2,1)S(1)} %get-tuple-element.18.damped_ref, bf16[8,128,128]{2,1,0:T(8,128)(2,1)S(1)} %all-to-all-done.1.state_ref, ...), custom_call_target="tpu_custom_call" | custom-call | flops 1073741824 | bytes 1048576 | tf_op jit(solution)/shard_map/pallas_call | solution.py:371
  87.0 2.7 %collective-permute-start.5 = (bf16[128,2048]{1,0:T(8,128)(2,1)S(1)}, bf16[128,2048]{1,0:T(8,128)(2,1)S(1)}, u32[]{:S(2)}, u32[]{:S(2)}) collective-permute-start(bf16[128,2048]{1,0:T(8,128)(2,1)S(1)} %get-tuple-element.22), channel_id=1, source_target_pairs={{0,1},{1,0},{2,3},{3,2},{4,5},{5,4},{6,7},{7,6},{8,9},{9,8},{10,11... | collective-permute-start | bytes 1572872 | tf_op jit(solution)/shard_map/ppermute | solution.py:514
  89.7 1.5 %collective-permute-done.5 = bf16[128,2048]{1,0:T(8,128)(2,1)S(1)} collective-permute-done((bf16[128,2048]{1,0:T(8,128)(2,1)S(1)}, bf16[128,2048]{1,0:T(8,128)(2,1)S(1)}, u32[]{:S(2)}, u32[]{:S(2)}) %collective-permute-start.5) | collective-permute-done | bytes 524320 | tf_op jit(solution)/shard_map/ppermute | solution.py:514
  91.2 0.9 fusion
  (2 shorter events, 0.1 us)
Async XLA Ops:
  4.1 25.3 %copy-start.9 = (bf16[512,512]{1,0:T(8,128)(2,1)S(1)}, bf16[512,512]{1,0:T(8,128)(2,1)}, u32[]{:S(2)}) copy-start(bf16[512,512]{1,0:T(8,128)(2,1)} %top_hbm.1) | copy-start | bytes 1572868
  27.3 16.2 %copy-start.10 = (bf16[256,512]{1,0:T(8,128)(2,1)S(1)}, bf16[256,512]{1,0:T(8,128)(2,1)}, u32[]{:S(2)}) copy-start(bf16[256,512]{1,0:T(8,128)(2,1)} %low_hbm.1) | copy-start | bytes 786436
  27.3 8.8 %collective-permute-start = (bf16[8,144,128]{2,1,0:T(8,128)(2,1)S(1)}, bf16[8,144,128]{2,1,0:T(8,128)(2,1)S(1)}, u32[]{:S(2)}, u32[]{:S(2)}) collective-permute-start(bf16[8,144,128]{2,1,0:T(8,128)(2,1)S(1)} %slice.4), channel_id=1, source_target_pairs={{0,56},{8,16},{16,8},{24,32},{32,24},{40,48},{48,40},{56,0},{1,57}... | collective-permute-start | bytes 884744 | tf_op jit(solution)/shard_map/ppermute | solution.py:472
  36.2 23.8 %copy-start.1 = (bf16[1,256,512]{2,1,0:T(8,128)(2,1)S(1)}, bf16[1,256,512]{2,1,0:T(8,128)(2,1)}, u32[]{:S(2)}) copy-start(bf16[1,256,512]{2,1,0:T(8,128)(2,1)} %param.16) | copy-start | bytes 786436
  36.2 23.8 %copy-start.2 = (bf16[1,256,512]{2,1,0:T(8,128)(2,1)S(1)}, bf16[1,256,512]{2,1,0:T(8,128)(2,1)}, u32[]{:S(2)}) copy-start(bf16[1,256,512]{2,1,0:T(8,128)(2,1)} %param.17) | copy-start | bytes 786436
  36.2 23.7 %copy-start.3 = (bf16[1,256,512]{2,1,0:T(8,128)(2,1)S(1)}, bf16[1,256,512]{2,1,0:T(8,128)(2,1)}, u32[]{:S(2)}) copy-start(bf16[1,256,512]{2,1,0:T(8,128)(2,1)} %param.15) | copy-start | bytes 786436
  36.2 23.7 %copy-start.5 = (f32[2,512]{1,0:T(2,128)S(1)}, f32[2,512]{1,0:T(2,128)}, u32[]{:S(2)}) copy-start(f32[2,512]{1,0:T(2,128)} %floor_ref.1) | copy-start | bytes 12292
  36.2 23.7 %copy-start.6 = (f32[1,256,4]{1,2,0:T(4,128)S(1)}, f32[1,256,4]{1,2,0:T(4,128)}, u32[]{:S(2)}) copy-start(f32[1,256,4]{1,2,0:T(4,128)} %param.19) | copy-start | bytes 12292
  36.2 29.9 %collective-permute-start.1 = (bf16[8,288,128]{2,1,0:T(8,128)(2,1)S(1)}, bf16[8,288,128]{2,1,0:T(8,128)(2,1)S(1)}, u32[]{:S(2)}, u32[]{:S(2)}) collective-permute-start(bf16[8,288,128]{2,1,0:T(8,128)(2,1)S(1)} %pad_maximum_fusion.pair_ref), channel_id=1, source_target_pairs={{0,1},{1,0},{2,3},{3,2},{4,5},{5,4},{6,7},{7,6},{8,9},{9,8},{10,11... | collective-permute-start | bytes 1769480 | tf_op jit(solution)/shard_map/ppermute | solution.py:473
  44.3 27.1 %collective-permute-start.2 = (bf16[768,512]{1,0:T(8,128)(2,1)}, bf16[768,512]{1,0:T(8,128)(2,1)S(1)}, u32[]{:S(2)}, u32[]{:S(2)}) collective-permute-start(bf16[768,512]{1,0:T(8,128)(2,1)} %constant_dynamic-update-slice_fusion), channel_id=1, source_target_pairs={{0,4},{2,6},{4,0},{6,2},{1,5},{3,7},{5,1},{7,3},{8,12},{10,14},{12... | collective-permute-start | bytes 2359304 | tf_op jit(solution)/shard_map/ppermute | solution.py:450
  49.2 35.2 %collective-permute-start.3 = (bf16[768,512]{1,0:T(8,128)(2,1)}, bf16[768,512]{1,0:T(8,128)(2,1)}, u32[]{:S(2)}, u32[]{:S(2)}) collective-permute-start(bf16[768,512]{1,0:T(8,128)(2,1)} %constant_dynamic-update-slice_fusion), channel_id=1, source_target_pairs={{0,2},{2,4},{4,6},{6,0},{1,3},{3,5},{5,7},{7,1},{8,10},{10,12},{12... | collective-permute-start | bytes 2359304 | tf_op jit(solution)/shard_map/ppermute | solution.py:448
  51.4 33.0 %collective-permute-start.4 = (bf16[768,512]{1,0:T(8,128)(2,1)}, bf16[768,512]{1,0:T(8,128)(2,1)}, u32[]{:S(2)}, u32[]{:S(2)}) collective-permute-start(bf16[768,512]{1,0:T(8,128)(2,1)} %constant_dynamic-update-slice_fusion), channel_id=1, source_target_pairs={{0,6},{2,0},{4,2},{6,4},{1,7},{3,1},{5,3},{7,5},{8,14},{10,8},{12,... | collective-permute-start | bytes 2359304 | tf_op jit(solution)/shard_map/ppermute | solution.py:449
  56.5 27.9 %all-to-all-start.1 = ((bf16[8,128,128]{2,1,0:T(8,128)(2,1)}), bf16[8,128,128]{2,1,0:T(8,128)(2,1)S(1)}, u32[]{:S(2)}, u32[]{:S(2)}) async-start(bf16[8,128,128]{2,1,0:T(8,128)(2,1)} %shard_map.162), calls=%async_computation.1 | async-start | bytes 524288 | tf_op jit(solution)/shard_map/all_to_all | solution.py:399
  60.0 5.6 %copy-start = (bf16[256,1024]{1,0:T(8,128)(2,1)S(1)}, bf16[256,1024]{1,0:T(8,128)(2,1)}, u32[]{:S(2)}) copy-start(bf16[256,1024]{1,0:T(8,128)(2,1)} %up_ref.3) | copy-start | bytes 1572868
  65.6 0.9 %copy-start.4 = (bf16[1,256,384]{2,1,0:T(8,128)(2,1)S(1)}, bf16[1,256,384]{2,1,0:T(8,128)(2,1)}, u32[]{:S(2)}) copy-start(bf16[1,256,384]{2,1,0:T(8,128)(2,1)} %param.21) | copy-start | bytes 589828
  65.6 1.0 %copy-start.7 = (f32[16,2048]{1,0:T(8,128)S(1)}, f32[16,2048]{1,0:T(8,128)}, u32[]{:S(2)}) copy-start(f32[16,2048]{1,0:T(8,128)} %constant.4.clone.cos_hbm.cos_ref) | copy-start | bytes 393220
  65.6 1.0 %copy-start.8 = (f32[16,2048]{1,0:T(8,128)S(1)}, f32[16,2048]{1,0:T(8,128)}, u32[]{:S(2)}) copy-start(f32[16,2048]{1,0:T(8,128)} %constant.5.clone.sin_hbm.sin_ref) | copy-start | bytes 393220
  87.0 4.2 %collective-permute-start.5 = (bf16[128,2048]{1,0:T(8,128)(2,1)S(1)}, bf16[128,2048]{1,0:T(8,128)(2,1)S(1)}, u32[]{:S(2)}, u32[]{:S(2)}) collective-permute-start(bf16[128,2048]{1,0:T(8,128)(2,1)S(1)} %get-tuple-element.22), channel_id=1, source_target_pairs={{0,1},{1,0},{2,3},{3,2},{4,5},{5,4},{6,7},{7,6},{8,9},{9,8},{10,11... | collective-permute-start | bytes 1572872 | tf_op jit(solution)/shard_map/ppermute | solution.py:514
